TPU v7x, 32 devices: a whole 2x2x4 slice. The times are simulated.
32 devices in a mesh: fs: 8 (over z, y), tp: 4 (over x, core).
Axes of the slice: x: 2, y: 2, z: 4, core: 2. Of those that a mesh axis runs over, the one named last changes fastest.
Arguments:
- tokens: bfloat16 [8192, 2048], P('fs', 'tp'), may hold values from -6 to 6
- mixer_gain: float32 [2048], replicated, may hold values from 0.1 to 1.9
- ffn_gain: float32 [2048], replicated, may hold values from 0.1 to 1.9
- w_outer: float32 [2048, 1024], P('fs', 'tp'), may hold values from -0.125 to 0.125
- w_inner: float32 [2048, 1024], P('fs', 'tp'), may hold values from -0.125 to 0.125
- w_value: float32 [2048, 1024], P('fs', 'tp'), may hold values from -0.125 to 0.125
- scale_outer: float32 [1, 1024], P(None, 'tp'), may hold values from 0.5 to 2
- scale_inner: float32 [1, 1024], P(None, 'tp'), may hold values from 0.5 to 2
- scale_value: float32 [1, 1024], P(None, 'tp'), may hold values from 0.5 to 2
- conv_taps: float32 [3, 1024], P(None, 'tp'), may hold values from -3.5 to 3.5
- w_mixout: float32 [1024, 2048], P('tp', 'fs'), may hold values from -0.1875 to 0.1875
- scale_mixout: float32 [1, 2048], P(None, 'fs'), may hold values from 0.5 to 2
- w_gate: float32 [2048, 5632], P('fs', 'tp'), may hold values from -0.125 to 0.125
- w_upward: float32 [2048, 5632], P('fs', 'tp'), may hold values from -0.125 to 0.125
- scale_gate: float32 [1, 5632], P(None, 'tp'), may hold values from 0.5 to 2
- scale_upward: float32 [1, 5632], P(None, 'tp'), may hold values from 0.5 to 2
- w_down: float32 [5632, 2048], P('tp', 'fs'), may hold values from -0.078125 to 0.078125
- scale_down: float32 [1, 2048], P(None, 'fs'), may hold values from 0.5 to 2
Outputs:
- block_out: bfloat16 [8192, 2048], P('fs', 'tp')
All inputs are finite; a program needn't handle non-finite values.
Results may differ from a plain program's by a relative error of at most 0.019.
Values may be sent and summed in bfloat16 or wider, within the bound.
A program may use at most 128 MiB of HBM per device.

v0:
```python
import jax
import jax.numpy as jnp
from jax import lax
from jax.experimental import pallas as pl
from jax.experimental.pallas import tpu as pltpu
from jax.sharding import PartitionSpec as P

SEQ_LEN = 128


def rms_scaled(full_rows, gain_vec):
    values = full_rows.astype(jnp.float32)
    inverse = lax.rsqrt(jnp.mean(values * values, axis=-1, keepdims=True) + 1e-06)
    return (values * inverse * gain_vec).astype(jnp.bfloat16)


def add_rows(left, w_piece):
    return jnp.dot(left, w_piece, preferred_element_type=jnp.float32)


def causal_taps(product, conv_taps):
    padded = jnp.pad(product, ((0, 0), (conv_taps.shape[0] - 1, 0), (0, 0)))
    length = product.shape[1]
    summed = jnp.zeros(product.shape, jnp.float32)
    for tap_index in range(conv_taps.shape[0]):
        summed = summed + conv_taps[tap_index] * padded[:, tap_index : tap_index + length, :]
    return summed


DEPTH, WIDTH, TP = 4, 2, 4
ROWS = 256
MESH = pl.DeviceIdType.MESH


def block_kernel(
    tokens, mixer_gain, ffn_gain, s_mixer, taps, s_gate, s_up,
    h_scales, h_mixer, h_mixout, h_gate, h_up, h_down,
    out, residual_own,
    rows, mixer, mixout, gate, up, down, scales, mixed, hidden,
    fs_send, fs_recv, tp_send, tp_recv, local_sem,
):
    f32, bf16 = jnp.float32, jnp.bfloat16
    me, tp = lax.axis_index("fs"), lax.axis_index("tp")
    zed, why = lax.div(me, WIDTH), lax.rem(me, WIDTH)
    near_x, core = lax.div(tp, 2), lax.rem(tp, 2)

    def at(dz, dy):
        return lax.rem(zed + dz + DEPTH, DEPTH) * WIDTH + lax.rem(why + dy, WIDTH)

    beside, above, below = at(0, 1), at(1, 0), at(-1, 0)
    sibling = near_x * 2 + (1 - core)
    across = (1 - near_x) * 2 + core

    barrier = pltpu.get_barrier_semaphore()
    for peer in (beside, above, below):
        pl.semaphore_signal(barrier, inc=1, device_id={"fs": peer}, device_id_type=MESH)
    for peer in (sibling, across):
        pl.semaphore_signal(barrier, inc=1, device_id={"tp": peer}, device_id_type=MESH)
    pl.semaphore_wait(barrier, 5)

    shards = (h_scales, h_mixer, h_mixout, h_gate, h_up, h_down)
    fulls = (scales, mixer, mixout, gate, up, down)
    by_columns = (False, False, True, False, False, True)

    def slot(w, owner, part):
        height, wide = shards[w].shape
        first, size = 0, height
        if part is not None:
            size = height // 2
            first = part * size
        if by_columns[w]:
            base = tp * height if w == 2 else 0
            start = base + first
            if w == 2:
                start = pl.multiple_of(start, 128)
            return fulls[w].at[pl.ds(start, size), pl.ds(pl.multiple_of(owner * wide, wide), wide)]
        return fulls[w].at[pl.ds(pl.multiple_of(owner * height + first, size), size), :]

    kinds = (
        ((0, 0), None, beside), ((0, 0), None, above), ((0, 0), None, below),
        ((0, 1), None, above), ((0, 1), None, below),
        ((-1, 0), 0, above), ((1, 0), 1, below),
        ((2, 0), 0, beside), ((2, 0), 1, beside),
    )

    def copy(w, k):
        (dz, dy), part, target = kinds[k]
        place = slot(w, at(dz, dy), part)
        return pltpu.make_async_remote_copy(
            src_ref=shards[w] if k < 3 else place,
            dst_ref=place,
            send_sem=fs_send.at[w, k],
            recv_sem=fs_recv.at[w, k],
            device_id={"fs": target},
            device_id_type=MESH,
        )

    def own(w):
        return pltpu.make_async_copy(shards[w], slot(w, me, None), local_sem.at[w])

    def first(w):
        for k in (0, 1, 2):
            copy(w, k).start()
        own(w).start()

    def second(w):
        copy(w, 1).wait_recv()
        copy(w, 5).start()
        copy(w, 2).wait_recv()
        copy(w, 6).start()
        copy(w, 0).wait_recv()
        copy(w, 3).start()
        copy(w, 4).start()

    def third(w):
        copy(w, 5).wait_recv()
        copy(w, 7).start()
        copy(w, 6).wait_recv()
        copy(w, 8).start()

    def finish(w):
        for k in (3, 4, 7, 8):
            copy(w, k).wait_recv()
        own(w).wait()

    def tp_slot(a, owner):
        if a == 0:
            wide = tokens.shape[1]
            return rows.at[:, pl.ds(pl.multiple_of(owner * wide, wide), wide)]
        if a == 1:
            wide = mixed.shape[1] // TP
            return mixed.at[:, pl.ds(pl.multiple_of(owner * wide, wide), wide)]
        height = mixout.shape[0] // TP
        return mixout.at[pl.ds(pl.multiple_of(owner * height, height), height), :]

    def tp_copy(a, k):
        owner, target = ((tp, sibling), (tp, across), (across, sibling))[k]
        place = tp_slot(a, owner)
        return pltpu.make_async_remote_copy(
            src_ref=tokens if a == 0 and k < 2 else place,
            dst_ref=place,
            send_sem=tp_send.at[a, k],
            recv_sem=tp_recv.at[a, k],
            device_id={"tp": target},
            device_id_type=MESH,
        )

    def tp_first(a):
        tp_copy(a, 1).start()
        tp_copy(a, 0).start()

    def tp_second(a):
        tp_copy(a, 1).wait_recv()
        tp_copy(a, 2).start()

    def tp_finish(a):
        tp_copy(a, 0).wait_recv()
        tp_copy(a, 2).wait_recv()

    own_tokens = pltpu.make_async_copy(tokens, tp_slot(0, tp), local_sem.at[6])
    tp_first(0)
    own_tokens.start()
    for w in (1, 2, 0, 3):
        first(w)
    second(1)
    second(2)
    second(0)
    first(4)
    third(1)
    third(2)
    third(0)
    second(3)
    first(5)
    tp_second(0)
    finish(2)
    tp_first(2)
    finish(1)
    tp_finish(0)
    own_tokens.wait()

    count = tokens.shape[0] // ROWS
    chan = mixed.shape[1] // TP

    def tile(i):
        return pl.ds(pl.multiple_of(i * ROWS, ROWS), ROWS)

    def normalised(values, gain):
        inverse = lax.rsqrt(jnp.mean(values * values, axis=-1, keepdims=True) + 1e-06)
        return (values * inverse * gain[...]).astype(bf16)

    @pl.loop(0, count)
    def _(i):
        normed = normalised(rows[tile(i), :].astype(f32), mixer_gain)
        three = jnp.dot(normed, mixer[...], preferred_element_type=f32) * s_mixer[...]
        product = three[:, chan : 2 * chan] * three[:, 2 * chan :]
        place = lax.rem(lax.broadcasted_iota(jnp.int32, product.shape, 0), SEQ_LEN)
        total = jnp.zeros_like(product)
        last = taps.shape[0] - 1
        for j in range(taps.shape[0]):
            back = last - j
            moved = product
            if back:
                moved = jnp.where(place >= back, pltpu.roll(product, back, 0), 0.0)
            total = total + taps[j : j + 1, :] * moved
        mixed[tile(i), pl.ds(pl.multiple_of(tp * chan, chan), chan)] = (
            three[:, :chan] * total
        ).astype(bf16)

    tp_first(1)
    third(3)
    second(4)
    tp_second(2)
    tp_second(1)
    finish(0)
    tp_finish(2)
    tp_finish(1)
    for k in range(3):
        tp_copy(0, k).wait_send()

    block = scales.shape[1]
    blocks = DEPTH * WIDTH

    def scale_row(which):
        return jnp.concatenate(
            [scales[b * 16 + which * 8 : b * 16 + which * 8 + 1, :] for b in range(blocks)], axis=1
        )

    feat = tokens.shape[1]

    @pl.loop(0, count)
    def _(i):
        term = jnp.dot(mixed[tile(i), :], mixout[...], preferred_element_type=f32) * scale_row(0)
        residual = (rows[tile(i), :].astype(f32) + term).astype(bf16)
        rows[tile(i), :] = residual
        residual_own[tile(i), :] = rows[tile(i), pl.ds(pl.multiple_of(tp * feat, feat), feat)]
        rows[tile(i), :] = normalised(residual.astype(f32), ffn_gain)

    third(4)
    second(5)
    finish(3)
    finish(4)

    @pl.loop(0, count)
    def _(i):
        gate_part = jnp.dot(rows[tile(i), :], gate[...], preferred_element_type=f32) * s_gate[...]
        up_part = jnp.dot(rows[tile(i), :], up[...], preferred_element_type=f32) * s_up[...]
        hidden[tile(i), :] = (gate_part / (1.0 + jnp.exp(-gate_part)) * up_part).astype(bf16)

    third(5)
    finish(5)

    @pl.loop(0, count)
    def _(i):
        term = jnp.dot(hidden[tile(i), :], down[...], preferred_element_type=f32) * scale_row(1)
        out[tile(i), :] = term.astype(bf16)

    for w in range(6):
        for k in range(9):
            copy(w, k).wait_send()
    for a in (1, 2):
        for k in range(3):
            tp_copy(a, k).wait_send()


def fused_device(
    tokens,
    mixer_gain,
    ffn_gain,
    w_outer,
    w_inner,
    w_value,
    scale_outer,
    scale_inner,
    scale_value,
    conv_taps,
    w_mixout,
    scale_mixout,
    w_gate,
    w_upward,
    scale_gate,
    scale_upward,
    w_down,
    scale_down,
):
    bf16 = jnp.bfloat16
    count, feat = tokens.shape
    model = mixer_gain.shape[0]
    chan = w_outer.shape[1]
    units = w_gate.shape[1]
    cols = w_down.shape[1]
    shard = jnp.concatenate([w_outer, w_inner, w_value], axis=1).astype(bf16)
    s_mixer = jnp.concatenate([scale_outer, scale_inner, scale_value], axis=1)
    scale_shard = jnp.concatenate(
        [jnp.broadcast_to(scale_mixout, (8, cols)), jnp.broadcast_to(scale_down, (8, cols))], axis=0
    )
    vmem = pl.BlockSpec(memory_space=pltpu.VMEM)
    dma = pltpu.SemaphoreType.DMA
    terms, residual = pl.pallas_call(
        block_kernel,
        out_shape=(
            jax.ShapeDtypeStruct((count, model), bf16),
            jax.ShapeDtypeStruct((count, feat), bf16),
        ),
        in_specs=[vmem] * 13,
        out_specs=(vmem, vmem),
        scratch_shapes=[
            pltpu.VMEM((count, model), bf16),
            pltpu.VMEM((model, 3 * chan), bf16),
            pltpu.VMEM((TP * chan, model), bf16),
            pltpu.VMEM((model, units), bf16),
            pltpu.VMEM((model, units), bf16),
            pltpu.VMEM((units, model), bf16),
            pltpu.VMEM((16 * DEPTH * WIDTH, cols), jnp.float32),
            pltpu.VMEM((count, TP * chan), bf16),
            pltpu.VMEM((count, units), bf16),
            dma((6, 9)),
            dma((6, 9)),
            dma((3, 3)),
            dma((3, 3)),
            dma((7,)),
        ],
        compiler_params=pltpu.CompilerParams(
            collective_id=0, has_side_effects=True, vmem_limit_bytes=62 * 1024 * 1024
        ),
    )(
        tokens, mixer_gain[None], ffn_gain[None], s_mixer, conv_taps, scale_gate, scale_upward,
        scale_shard, shard, w_mixout.astype(bf16), w_gate.astype(bf16), w_upward.astype(bf16),
        w_down.astype(bf16),
    )
    share = lax.psum_scatter(terms, "tp", scatter_dimension=1, tiled=True)
    return (residual.astype(jnp.float32) + share.astype(jnp.float32)).astype(bf16)


def plain_device(
    tokens,
    mixer_gain,
    ffn_gain,
    w_outer,
    w_inner,
    w_value,
    scale_outer,
    scale_inner,
    scale_value,
    conv_taps,
    w_mixout,
    scale_mixout,
    w_gate,
    w_upward,
    scale_gate,
    scale_upward,
    w_down,
    scale_down,
):
    full_rows = lax.all_gather(tokens, "tp", axis=1, tiled=True)
    normed = rms_scaled(full_rows, mixer_gain)
    tok_count = tokens.shape[0]
    local_channels = w_outer.shape[1]

    def add_one(w_piece):
        return add_rows(normed, w_piece)

    outer_bf = w_outer.astype(jnp.bfloat16)
    inner_bf = w_inner.astype(jnp.bfloat16)
    value_bf = w_value.astype(jnp.bfloat16)
    outer = add_one(lax.all_gather(outer_bf, "fs", axis=0, tiled=True))
    inner = add_one(lax.all_gather(inner_bf, "fs", axis=0, tiled=True))
    value = add_one(lax.all_gather(value_bf, "fs", axis=0, tiled=True))
    outer = outer * scale_outer
    product = inner * scale_inner * (value * scale_value)
    product = product.reshape(tok_count // SEQ_LEN, SEQ_LEN, local_channels)
    conv = causal_taps(product, conv_taps).reshape(tok_count, local_channels)
    mixed_out = (outer * conv).astype(jnp.bfloat16)
    mixout_scales, down_scales = (
        lax.all_gather(scale_mixout, "fs", axis=1, tiled=True),
        lax.all_gather(scale_down, "fs", axis=1, tiled=True),
    )
    mixout_bf = w_mixout.astype(jnp.bfloat16)
    mixed_all = lax.all_gather(mixed_out, "tp", axis=1, tiled=True)
    mixout_cols = lax.all_gather(mixout_bf, "fs", axis=1, tiled=True)
    mixout_all = lax.all_gather(mixout_cols, "tp", axis=0, tiled=True)
    mix_term = jnp.dot(mixed_all, mixout_all, preferred_element_type=jnp.float32) * mixout_scales
    residual_rows = (full_rows.astype(jnp.float32) + mix_term).astype(jnp.bfloat16)
    feature_count = tokens.shape[1]
    residual = lax.dynamic_slice_in_dim(
        residual_rows, lax.axis_index("tp") * feature_count, feature_count, 1
    )
    normed_ffn = rms_scaled(residual_rows, ffn_gain)
    gate_proj = add_rows(
        normed_ffn, lax.all_gather(w_gate.astype(jnp.bfloat16), "fs", axis=0, tiled=True)
    )
    up_proj = add_rows(
        normed_ffn, lax.all_gather(w_upward.astype(jnp.bfloat16), "fs", axis=0, tiled=True)
    )
    hidden = (jax.nn.silu(gate_proj * scale_gate) * (up_proj * scale_upward)).astype(jnp.bfloat16)
    down_terms = (
        jnp.dot(
            hidden,
            lax.all_gather(w_down.astype(jnp.bfloat16), "fs", axis=1, tiled=True),
            preferred_element_type=jnp.float32,
        )
        * down_scales
    )
    ffn_share = lax.psum_scatter(
        down_terms.astype(jnp.bfloat16), "tp", scatter_dimension=1, tiled=True
    ).astype(jnp.float32)
    return (residual.astype(jnp.float32) + ffn_share).astype(jnp.bfloat16)


def solution(mesh):
    in_specs = (
        P("fs", "tp"),
        P(),
        P(),
        P("fs", "tp"),
        P("fs", "tp"),
        P("fs", "tp"),
        P(None, "tp"),
        P(None, "tp"),
        P(None, "tp"),
        P(None, "tp"),
        P("tp", "fs"),
        P(None, "fs"),
        P("fs", "tp"),
        P("fs", "tp"),
        P(None, "tp"),
        P(None, "tp"),
        P("tp", "fs"),
        P(None, "fs"),
    )
    out_specs = P("fs", "tp")
    chosen = fused_device if (mesh.shape["fs"], mesh.shape["tp"]) == (8, 4) else plain_device
    return jax.shard_map(
        chosen, mesh=mesh, in_specs=in_specs, out_specs=out_specs, check_vma=False
    )
```

profile of v0, /device:TPU:3, one launch (start us, length us, event | category | flops | bytes accessed | tf_op | source)
XLA Modules:
  0.0 377.6 jit_solution(11508268790806069277)
XLA Ops:
  6.5 0.0 copy-start
  6.5 0.0 copy-start.1
  6.5 0.0 reduce-scatter.2.cloned.1.call-start
  6.5 1.1 convert.9
  7.7 1.0 convert.10
  8.6 1.0 convert.11
  9.6 1.6 convert_element_type.22.h_mixout
  11.2 0.0 copy-done
  11.2 0.0 copy-start.2
  11.2 0.9 convert_element_type.23.h_gate
  12.2 0.0 copy-done.1
  12.2 0.0 copy-start.4
  12.2 0.0 copy-start.5
  12.2 0.0 copy-start.6
  12.2 0.0 copy-start.7
  12.2 0.0 copy-start.8
  12.2 1.0 convert_element_type.24.h_up
  13.2 0.0 copy-done.2
  13.2 0.9 convert_element_type.25.h_down
  14.1 0.0 copy-done.4
  14.1 0.0 copy-done.5
  14.1 0.6 pad_maximum_fusion.1.h_scales
  14.7 0.0 copy-done.6
  14.7 0.0 copy-done.7
  14.7 0.0 copy-done.8
  14.7 0.6 pad_maximum_fusion.2.s_mixer
  15.3 0.8 pad_maximum_fusion.h_mixer
  16.1 305.4 %shard_map.172 = (bf16[1024,2048]{1,0:T(8,128)(2,1)}, bf16[1024,512]{1,0:T(8,128)(2,1)}) custom-call(bf16[1024,512]{1,0:T(8,128)(2,1)} %tokens.1, f32[1,2048]{1,0:T(1,128)} %bitcast.4, f32[1,2048]{1,0:T(1,128)} %bitcast.5, f32[1,768]{1,0:T(1,128)} %pad_maximum_fusion.2.s_mixer, f32[3,256]{1,0:T(4,128)} %taps.1, f32[1,1408]{1,0:T(1,128)} %s_gate.1, ...), custom_call_target="tpu_custom_call" | custom-call | tf_op jit(solution)/shard_map/pallas_call | solution.py:298
  321.5 0.0 copy-start.3
  321.5 0.0 reduce-scatter.2.cloned.1.call-update
  321.6 46.7 %reduce-scatter.2.cloned.1.call-done = bf16[1024,512]{1,0:T(8,128)(2,1)} async-done(((bf16[1024,2048]{1,0:T(8,128)(2,1)}), bf16[1024,512]{1,0:T(8,128)(2,1)}) %reduce-scatter.2.cloned.1.call-update) | async-done | bytes 1048592 | tf_op jit(solution)/shard_map/reduce_scatter | solution.py:330
  368.2 0.0 copy-done.3
  368.2 2.5 add_convert_fusion
  (2 shorter events, 0.0 us)
Async XLA Ops:
  6.5 4.7 %copy-start = (f32[256,1408]{1,0:T(8,128)S(1)}, f32[256,1408]{1,0:T(8,128)}, u32[]{:S(2)}) copy-start(f32[256,1408]{1,0:T(8,128)} %param.30) | copy-start | bytes 4325380
  6.5 5.6 %copy-start.1 = (f32[256,1408]{1,0:T(8,128)S(1)}, f32[256,1408]{1,0:T(8,128)}, u32[]{:S(2)}) copy-start(f32[256,1408]{1,0:T(8,128)} %param.31) | copy-start | bytes 4325380
  6.5 361.7 %reduce-scatter.2.cloned.1.call-start = ((), (), s32[]{:S(2)}) async-start(), calls=%async_computation.1 | async-start | bytes 5242880 | tf_op jit(solution)/shard_map/reduce_scatter | solution.py:330
  11.2 1.9 copy-start.2
  12.2 1.9 copy-start.4
  12.2 1.9 copy-start.5
  12.2 2.6 copy-start.6
  12.2 2.6 copy-start.7
  12.2 2.5 copy-start.8
  321.5 46.7 %copy-start.3 = (bf16[1024,512]{1,0:T(8,128)(2,1)S(1)}, bf16[1024,512]{1,0:T(8,128)(2,1)}, u32[]{:S(2)}) copy-start(bf16[1024,512]{1,0:T(8,128)(2,1)} %get-tuple-element.7) | copy-start | bytes 3145732
Sparse Core Ops, SparseCore 0:
  321.7 46.5 reduce-scatter.1
where the time goes:
time: 380 us; the launch traced here: 378 us
  Pallas kernels  305 us (80%)
  waiting for transfers between devices  46.7 us (12%)
  between operations  13.4 us (4%)
  other arithmetic  12 us (3%)
    pallas_call x1, Pallas kernels, fused_device(): pl.pallas_call(block_kernel, out_shape=(jax.ShapeDtypeStruct((count, mode...  305 us
    reduce_scatter x1, waiting for transfers between devices, fused_device(): share = lax.psum_scatter(terms, 'tp', scatter_dimension=1, tiled=True)  46.7 us
  transfers between devices with their start and end apart: 1, of which 1 were waited for; matrix products, arithmetic and copies ran while one was open for 0% of the time, Pallas kernels for 0%

commit v1 on v0

v1 whole, which is shorter than its diff:
```python
import jax
import jax.numpy as jnp
from jax import lax
from jax.experimental import pallas as pl
from jax.experimental.pallas import tpu as pltpu
from jax.sharding import PartitionSpec as P

SEQ_LEN = 128


def rms_scaled(full_rows, gain_vec):
    values = full_rows.astype(jnp.float32)
    inverse = lax.rsqrt(jnp.mean(values * values, axis=-1, keepdims=True) + 1e-06)
    return (values * inverse * gain_vec).astype(jnp.bfloat16)


def add_rows(left, w_piece):
    return jnp.dot(left, w_piece, preferred_element_type=jnp.float32)


def causal_taps(product, conv_taps):
    padded = jnp.pad(product, ((0, 0), (conv_taps.shape[0] - 1, 0), (0, 0)))
    length = product.shape[1]
    summed = jnp.zeros(product.shape, jnp.float32)
    for tap_index in range(conv_taps.shape[0]):
        summed = summed + conv_taps[tap_index] * padded[:, tap_index : tap_index + length, :]
    return summed


DEPTH, WIDTH, TP = 4, 2, 4
ROWS = 256
PIECE = 512
UP, DOWN = 0, 1
SCALES, MIXER, MIXOUT, GATED, BACK = range(5)
MESH = pl.DeviceIdType.MESH


def block_kernel(
    tokens, mixer_gain, ffn_gain, s_mixer, taps, s_gated,
    h_scales, h_mixer, h_mixout, h_gated, h_back,
    out,
    act, mixer, mixout, gated, back, scales, mixed, hidden, residual_own,
    part, from_core, from_y, from_x,
    z_send, y_send, fs_recv, tp_send, tp_recv, mx_send, mx_recv,
    act_send, act_recv, core_send, core_recv, sum_send, sum_recv, last_send, last_recv,
    local_sem,
):
    f32, bf16 = jnp.float32, jnp.bfloat16
    me, tp = lax.axis_index("fs"), lax.axis_index("tp")
    zed, why = lax.div(me, WIDTH), lax.rem(me, WIDTH)
    ex, core = lax.div(tp, 2), lax.rem(tp, 2)
    other = 1 - why
    last_z = DEPTH - 1
    count = tokens.shape[0]
    tiles = count // ROWS

    beside = zed * WIDTH + other
    sibling = ex * 2 + (1 - core)
    across = (1 - ex) * 2 + core

    barrier = pltpu.get_barrier_semaphore()
    ring = [lax.rem(zed + step, DEPTH) * WIDTH + why for step in (1, DEPTH - 1)]
    for peer in (beside, *ring):
        pl.semaphore_signal(barrier, inc=1, device_id={"fs": peer}, device_id_type=MESH)
    for peer in (sibling, across):
        pl.semaphore_signal(barrier, inc=1, device_id={"tp": peer}, device_id_type=MESH)
    pl.semaphore_wait(barrier, 5)

    fulls = (scales, mixer, mixout, gated, back)
    own_src = (h_scales, h_mixer, h_mixout, h_gated.at[why], h_back.at[why])

    def place(p, owner):
        if p in (MIXER, GATED):
            height = own_src[p].shape[0]
            return fulls[p].at[pl.ds(pl.multiple_of(owner * height, height), height), :]
        height, wide = own_src[p].shape
        first = pl.multiple_of(tp * height, height) if p == MIXOUT else 0
        return fulls[p].at[pl.ds(first, height), pl.ds(pl.multiple_of(owner * wide, wide), wide)]

    def z_copy(p, owner, way, src=None):
        spot = place(p, owner)
        step = 1 if way == UP else -1
        return pltpu.make_async_remote_copy(
            src_ref=spot if src is None else src,
            dst_ref=spot,
            send_sem=z_send.at[p, owner, way],
            recv_sem=fs_recv.at[p, owner],
            device_id={"fs": (zed + step) * WIDTH + why},
            device_id_type=MESH,
        )

    def y_copy(p, owner, src=None):
        spot = place(p, owner)
        return pltpu.make_async_remote_copy(
            src_ref=spot if src is None else src,
            dst_ref=spot,
            send_sem=y_send.at[p, owner],
            recv_sem=fs_recv.at[p, owner],
            device_id={"fs": beside},
            device_id_type=MESH,
        )

    def arrived(p, owner):
        y_copy(p, owner).wait_recv()

    def own(p):
        return pltpu.make_async_copy(own_src[p], place(p, me), local_sem.at[p])

    can_up, can_down = zed < last_z, zed > 0
    outer = (zed == 0) | (zed == last_z)

    def z_own(p, row, src):
        owner = zed * WIDTH + row
        pl.when(can_up)(lambda: z_copy(p, owner, UP, src).start())
        pl.when(can_down)(lambda: z_copy(p, owner, DOWN, src).start())

    def relay(p, s, row):
        low, high = (zed - s) * WIDTH + row, (zed + s) * WIDTH + row

        @pl.when((zed >= s) & can_up)
        def _():
            arrived(p, low)
            z_copy(p, low, UP).start()

        @pl.when((zed + s <= last_z) & can_down)
        def _():
            arrived(p, high)
            z_copy(p, high, DOWN).start()

    def settle(p, s, row):
        low, high = (zed - s) * WIDTH + row, (zed + s) * WIDTH + row
        pl.when((zed >= s) & (zed == last_z))(lambda: arrived(p, low))
        pl.when((zed + s <= last_z) & (zed == 0))(lambda: arrived(p, high))

    def mx_copy(owner, k, src=None):
        line, target = ((tp, sibling), (tp, across), (across, sibling))[k]
        height, wide = h_mixout.shape
        spot = mixout.at[
            pl.ds(pl.multiple_of(line * height, height), height),
            pl.ds(pl.multiple_of(owner * wide, wide), wide),
        ]
        return pltpu.make_async_remote_copy(
            src_ref=spot if src is None else src,
            dst_ref=spot,
            send_sem=mx_send.at[owner, k],
            recv_sem=mx_recv.at[owner, k],
            device_id={"tp": target},
            device_id_type=MESH,
        )

    def mx_first(owner, src=None):
        mx_copy(owner, 1, src).start()
        mx_copy(owner, 0, src).start()

    firsts = (SCALES, MIXOUT, MIXER)

    def relay_first(s):
        low, high = (zed - s) * WIDTH + why, (zed + s) * WIDTH + why

        @pl.when(zed >= s)
        def _():
            for p in firsts:
                arrived(p, low)
                pl.when(can_up)(lambda: z_copy(p, low, UP).start())
                y_copy(p, low).start()
                if p == MIXOUT:
                    mx_first(low)

        @pl.when(zed + s <= last_z)
        def _():
            for p in firsts:
                arrived(p, high)
                pl.when(can_down)(lambda: z_copy(p, high, DOWN).start())
                y_copy(p, high).start()
                if p == MIXOUT:
                    mx_first(high)

    def from_beside(s):
        def take(owner):
            for p in firsts:
                arrived(p, owner)
                if p == MIXOUT:
                    mx_first(owner)

        if s == 0:
            take(beside)
            return
        low, high = (zed - s) * WIDTH + other, (zed + s) * WIDTH + other
        pl.when(zed >= s)(lambda: take(low))
        pl.when(zed + s <= last_z)(lambda: take(high))

    base = pl.multiple_of(why * count, count)

    def tp_slot(a, owner):
        if a == 0:
            wide = tokens.shape[1]
            return act.at[pl.ds(base, count), pl.ds(pl.multiple_of(owner * wide, wide), wide)]
        wide = mixed.shape[1] // TP
        return mixed.at[:, pl.ds(pl.multiple_of(owner * wide, wide), wide)]

    def tp_copy(a, k):
        owner, target = ((tp, sibling), (tp, across), (across, sibling))[k]
        spot = tp_slot(a, owner)
        return pltpu.make_async_remote_copy(
            src_ref=tokens if a == 0 and k < 2 else spot,
            dst_ref=spot,
            send_sem=tp_send.at[a, k],
            recv_sem=tp_recv.at[a, k],
            device_id={"tp": target},
            device_id_type=MESH,
        )

    def tp_first(a):
        tp_copy(a, 1).start()
        tp_copy(a, 0).start()

    def tp_second(a):
        tp_copy(a, 1).wait_recv()
        tp_copy(a, 2).start()

    def tp_finish(a):
        tp_copy(a, 0).wait_recv()
        tp_copy(a, 2).wait_recv()

    own_tokens = pltpu.make_async_copy(tokens, tp_slot(0, tp), local_sem.at[5])

    for p in firsts:
        y_copy(p, me, own_src[p]).start()
        z_own(p, why, own_src[p])
    tp_first(0)
    mx_first(me, h_mixout)
    own_tokens.start()
    for p in range(5):
        own(p).start()
    units = h_back.shape[1]
    back[units:, :] = jnp.zeros((back.shape[0] - units, back.shape[1]), bf16)

    relay_first(1)
    tp_second(0)
    relay_first(2)
    z_own(GATED, why, own_src[GATED])
    relay_first(3)
    for p in (GATED, BACK):
        y_copy(p, me, (h_gated if p == GATED else h_back).at[other]).start()
    for s in range(DEPTH):
        from_beside(s)
    relay(GATED, 1, why)
    tp_finish(0)
    own_tokens.wait()
    for p in firsts:
        own(p).wait()

    chan = mixed.shape[1] // TP

    def tile(i):
        return pl.ds(pl.multiple_of(i * ROWS, ROWS), ROWS)

    def own_rows(i):
        return pl.ds(pl.multiple_of(base + i * ROWS, ROWS), ROWS)

    def normalised(values, gain):
        inverse = lax.rsqrt(jnp.mean(values * values, axis=-1, keepdims=True) + 1e-06)
        return (values * inverse * gain[...]).astype(bf16)

    @pl.loop(0, tiles)
    def _(i):
        normed = normalised(act[own_rows(i), :].astype(f32), mixer_gain)
        three = jnp.dot(normed, mixer[...], preferred_element_type=f32) * s_mixer[...]
        product = three[:, chan : 2 * chan] * three[:, 2 * chan :]
        row = lax.rem(lax.broadcasted_iota(jnp.int32, product.shape, 0), SEQ_LEN)
        total = jnp.zeros_like(product)
        last = taps.shape[0] - 1
        for j in range(taps.shape[0]):
            gap = last - j
            moved = product
            if gap:
                moved = jnp.where(row >= gap, pltpu.roll(product, gap, 0), 0.0)
            total = total + taps[j : j + 1, :] * moved
        mixed[tile(i), pl.ds(pl.multiple_of(tp * chan, chan), chan)] = (
            three[:, :chan] * total
        ).astype(bf16)

    tp_first(1)
    relay(GATED, 2, why)
    arrived(GATED, beside)
    z_own(GATED, other, None)
    for owner in range(DEPTH * WIDTH):
        mx_copy(owner, 1).wait_recv()
        mx_copy(owner, 2).start()
    tp_second(1)
    relay(GATED, 1, other)
    for owner in range(DEPTH * WIDTH):
        mx_copy(owner, 0).wait_recv()
        mx_copy(owner, 2).wait_recv()
    tp_finish(1)
    for k in range(3):
        tp_copy(0, k).wait_send()

    feat = tokens.shape[1]
    share = tiles // 2

    def act_copy(half, lead, q, k):
        spot = act.at[
            pl.ds(pl.multiple_of(half * count + (lead * share + q) * ROWS, ROWS), ROWS), :
        ]
        return pltpu.make_async_remote_copy(
            src_ref=spot,
            dst_ref=spot,
            send_sem=act_send.at[q, k],
            recv_sem=act_recv.at[q, k],
            device_id={"fs": beside} if k == 0 else {"tp": sibling},
            device_id_type=MESH,
        )

    @pl.loop(0, tiles)
    def _(step):
        i = lax.rem(step + core * share, tiles)
        term = jnp.dot(mixed[tile(i), :], mixout[...], preferred_element_type=f32)
        term = term * scales[0:1, :]
        residual = (act[own_rows(i), :].astype(f32) + term).astype(bf16)
        act[own_rows(i), :] = residual
        residual_own[tile(i), :] = act[
            own_rows(i), pl.ds(pl.multiple_of(tp * feat, feat), feat)
        ]
        act[own_rows(i), :] = normalised(residual.astype(f32), ffn_gain)
        pl.when(step < share)(lambda: act_copy(why, core, step, 0).start())

    z_own(BACK, why, own_src[BACK])
    arrived(BACK, beside)
    z_own(BACK, other, None)
    relay(GATED, 2, other)
    for row in (why, other):
        for s in (1, 2):
            relay(BACK, s, row)
    for q in range(share):
        act_copy(other, core, q, 0).wait_recv()
        act_copy(other, core, q, 1).start()
    own(GATED).wait()
    for row in (why, other):
        for s in (1, 2, 3):
            settle(GATED, s, row)

    main = (gated.shape[1] // 256) * 128

    def activate(first, steps):
        @pl.loop(0, steps)
        def _(i):
            rows = pl.ds(pl.multiple_of(first + i * ROWS, ROWS), ROWS)
            both = jnp.dot(act[rows, :], gated[...], preferred_element_type=f32)
            both = both * s_gated[pl.ds(why, 1), :]
            gate, up = both[:, :main], both[:, main + 128 :]
            hidden[rows, :main] = (gate / (1.0 + jnp.exp(-gate)) * up).astype(bf16)
            gate = both[:, main : main + 128]
            up = pltpu.roll(gate, 64, 1)
            rest = gate / (1.0 + jnp.exp(-gate)) * up
            lane = lax.broadcasted_iota(jnp.int32, rest.shape, 1)
            hidden[rows, main:] = jnp.where(lane < 64, rest, 0.0).astype(bf16)

    activate(base, tiles)
    for q in range(share):
        act_copy(other, 1 - core, q, 1).wait_recv()
    activate(other * count, tiles)

    own(BACK).wait()
    pieces = count // PIECE

    def piece(t):
        return pl.ds(pl.multiple_of(t * PIECE, PIECE), PIECE)

    def block_at(k):
        return lax.rem(zed + k * (1 - 2 * lax.div(zed, last_z)) + DEPTH, DEPTH)

    def core_copy(j, t):
        line = lax.div(j, 2)
        return pltpu.make_async_remote_copy(
            src_ref=part.at[j, piece(t), :],
            dst_ref=from_core.at[line, piece(t), :],
            send_sem=core_send.at[line, t],
            recv_sem=core_recv.at[line, t],
            device_id={"tp": sibling},
            device_id_type=MESH,
        )

    def sum_copy(j, q):
        line = lax.div(j, 2)
        return pltpu.make_async_remote_copy(
            src_ref=part.at[j, piece(other * pieces + q), :],
            dst_ref=from_y.at[line, piece(q), :],
            send_sem=sum_send.at[line, q],
            recv_sem=sum_recv.at[line, q],
            device_id={"fs": beside},
            device_id_type=MESH,
        )

    def last_copy(j, q):
        return pltpu.make_async_remote_copy(
            src_ref=part.at[j, piece(why * pieces + q), :],
            dst_ref=from_x.at[piece(q), :],
            send_sem=last_send.at[q],
            recv_sem=last_recv.at[q],
            device_id={"tp": across},
            device_id_type=MESH,
        )

    def multiply(k):
        j = block_at(k)
        if k:
            for row in range(WIDTH):
                pl.when(outer)(lambda: arrived(BACK, j * WIDTH + row))
        columns = pl.ds(pl.multiple_of(j * feat, feat), feat)

        @pl.loop(0, WIDTH * pieces)
        def _(step):
            t = lax.rem(step + other * pieces, WIDTH * pieces)
            term = jnp.dot(hidden[piece(t), :], back[:, columns], preferred_element_type=f32)
            part[j, piece(t), :] = (term * scales[8:9, columns]).astype(bf16)
            pl.when(core != lax.rem(j, 2))(lambda: core_copy(j, t).start())

    def added(j, t, extra):
        return part[j, piece(t), :].astype(f32) + extra.astype(f32)

    def reduce_core(k):
        j = block_at(k)

        @pl.when(core == lax.rem(j, 2))
        def _():
            line = lax.div(j, 2)
            for half in (other, why):
                for q in range(pieces):
                    t = half * pieces + q
                    core_copy(j, t).wait_recv()
                    part[j, piece(t), :] = added(j, t, from_core[line, piece(t), :]).astype(bf16)
                    if half is other:
                        sum_copy(j, q).start()

    def reduce_y(k):
        j = block_at(k)

        @pl.when(core == lax.rem(j, 2))
        def _():
            line = lax.div(j, 2)
            for q in range(pieces):
                t = why * pieces + q
                sum_copy(j, q).wait_recv()
                part[j, piece(t), :] = added(j, t, from_y[line, piece(q), :]).astype(bf16)
                pl.when(ex != line)(lambda: last_copy(j, q).start())

    def reduce_x(k):
        j = block_at(k)

        @pl.when(tp == j)
        def _():
            for q in range(pieces):
                t = why * pieces + q
                last_copy(j, q).wait_recv()
                total = added(j, t, from_x[piece(q), :])
                out[piece(q), :] = (residual_own[piece(q), :].astype(f32) + total).astype(bf16)

    for k in range(DEPTH):
        multiply(k)
        reduce_core(k)
        if k > 0:
            reduce_y(k - 1)
        if k > 1:
            reduce_x(k - 2)
    reduce_y(DEPTH - 1)
    reduce_x(DEPTH - 2)
    reduce_x(DEPTH - 1)

    def sent(p, row):
        owner = zed * WIDTH + row
        pl.when(can_up)(lambda: z_copy(p, owner, UP).wait_send())
        pl.when(can_down)(lambda: z_copy(p, owner, DOWN).wait_send())
        for s in (1, 2):
            low, high = (zed - s) * WIDTH + row, (zed + s) * WIDTH + row
            pl.when((zed >= s) & can_up)(lambda: z_copy(p, low, UP).wait_send())
            pl.when((zed + s <= last_z) & can_down)(lambda: z_copy(p, high, DOWN).wait_send())

    for p in range(5):
        sent(p, why)
        y_copy(p, me).wait_send()
        if p in (GATED, BACK):
            sent(p, other)
        else:
            for s in (1, 2, 3):
                low, high = (zed - s) * WIDTH + why, (zed + s) * WIDTH + why
                pl.when(zed >= s)(lambda: y_copy(p, low).wait_send())
                pl.when(zed + s <= last_z)(lambda: y_copy(p, high).wait_send())
    for owner in range(DEPTH * WIDTH):
        for k in range(3):
            mx_copy(owner, k).wait_send()
    for k in range(3):
        tp_copy(1, k).wait_send()
    for q in range(share):
        act_copy(why, core, q, 0).wait_send()
        act_copy(other, core, q, 1).wait_send()
    for j in range(DEPTH):

        @pl.when(core != j % 2)
        def _():
            for t in range(WIDTH * pieces):
                core_copy(j, t).wait_send()

        @pl.when(core == j % 2)
        def _():
            for q in range(pieces):
                sum_copy(j, q).wait_send()
                pl.when(ex != j // 2)(lambda: last_copy(j, q).wait_send())


def halves(gate, up, axis_units):
    half = axis_units // 2
    main = half // 128 * 128
    end = axis_units - main
    return jnp.stack(
        [
            jnp.concatenate(
                [gate[:, :main], gate[:, main:half], up[:, main:half], up[:, :main]], axis=1
            ),
            jnp.concatenate(
                [gate[:, end:], gate[:, half:end], up[:, half:end], up[:, end:]], axis=1
            ),
        ]
    )


def fused_device(
    tokens,
    mixer_gain,
    ffn_gain,
    w_outer,
    w_inner,
    w_value,
    scale_outer,
    scale_inner,
    scale_value,
    conv_taps,
    w_mixout,
    scale_mixout,
    w_gate,
    w_upward,
    scale_gate,
    scale_upward,
    w_down,
    scale_down,
):
    bf16 = jnp.bfloat16
    count, feat = tokens.shape
    model = mixer_gain.shape[0]
    chan = w_outer.shape[1]
    units = w_gate.shape[1]
    cols = w_down.shape[1]
    half = units // 2
    main = half // 128 * 128
    padded = main + 128
    shard = jnp.concatenate([w_outer, w_inner, w_value], axis=1).astype(bf16)
    s_mixer = jnp.concatenate([scale_outer, scale_inner, scale_value], axis=1)
    scale_shard = jnp.concatenate(
        [jnp.broadcast_to(scale_mixout, (8, cols)), jnp.broadcast_to(scale_down, (8, cols))], axis=0
    )
    h_gated = halves(w_gate.astype(bf16), w_upward.astype(bf16), units)
    s_gated = halves(scale_gate, scale_upward, units)[:, 0]
    w_back = w_down.astype(bf16)
    h_back = jnp.stack(
        [w_back[:half], jnp.concatenate([w_back[units - main :], w_back[half : units - main]])]
    )
    vmem = pl.BlockSpec(memory_space=pltpu.VMEM)
    dma = pltpu.SemaphoreType.DMA
    owners = DEPTH * WIDTH
    return pl.pallas_call(
        block_kernel,
        out_shape=jax.ShapeDtypeStruct((count, feat), bf16),
        in_specs=[vmem] * 11,
        out_specs=vmem,
        scratch_shapes=[
            pltpu.VMEM((WIDTH * count, model), bf16),
            pltpu.VMEM((model, 3 * chan), bf16),
            pltpu.VMEM((TP * chan, model), bf16),
            pltpu.VMEM((model, units), bf16),
            pltpu.VMEM((padded, model), bf16),
            pltpu.VMEM((16, model), jnp.float32),
            pltpu.VMEM((count, TP * chan), bf16),
            pltpu.VMEM((WIDTH * count, padded), bf16),
            pltpu.VMEM((count, feat), bf16),
            pltpu.VMEM((DEPTH, WIDTH * count, feat), bf16),
            pltpu.VMEM((2, WIDTH * count, feat), bf16),
            pltpu.VMEM((2, count, feat), bf16),
            pltpu.VMEM((count, feat), bf16),
            dma((5, owners, 2)),
            dma((5, owners)),
            dma((5, owners)),
            dma((2, 3)),
            dma((2, 3)),
            dma((owners, 3)),
            dma((owners, 3)),
            dma((2, 2)),
            dma((2, 2)),
            dma((2, 4)),
            dma((2, 4)),
            dma((2, 2)),
            dma((2, 2)),
            dma((2,)),
            dma((2,)),
            dma((6,)),
        ],
        compiler_params=pltpu.CompilerParams(
            collective_id=0, has_side_effects=True, vmem_limit_bytes=62 * 1024 * 1024
        ),
    )(
        tokens, mixer_gain[None], ffn_gain[None], s_mixer, conv_taps, s_gated,
        scale_shard, shard, w_mixout.astype(bf16), h_gated, h_back,
    )


def plain_device(
    tokens,
    mixer_gain,
    ffn_gain,
    w_outer,
    w_inner,
    w_value,
    scale_outer,
    scale_inner,
    scale_value,
    conv_taps,
    w_mixout,
    scale_mixout,
    w_gate,
    w_upward,
    scale_gate,
    scale_upward,
    w_down,
    scale_down,
):
    full_rows = lax.all_gather(tokens, "tp", axis=1, tiled=True)
    normed = rms_scaled(full_rows, mixer_gain)
    tok_count = tokens.shape[0]
    local_channels = w_outer.shape[1]

    def add_one(w_piece):
        return add_rows(normed, w_piece)

    outer_bf = w_outer.astype(jnp.bfloat16)
    inner_bf = w_inner.astype(jnp.bfloat16)
    value_bf = w_value.astype(jnp.bfloat16)
    outer = add_one(lax.all_gather(outer_bf, "fs", axis=0, tiled=True))
    inner = add_one(lax.all_gather(inner_bf, "fs", axis=0, tiled=True))
    value = add_one(lax.all_gather(value_bf, "fs", axis=0, tiled=True))
    outer = outer * scale_outer
    product = inner * scale_inner * (value * scale_value)
    product = product.reshape(tok_count // SEQ_LEN, SEQ_LEN, local_channels)
    conv = causal_taps(product, conv_taps).reshape(tok_count, local_channels)
    mixed_out = (outer * conv).astype(jnp.bfloat16)
    mixout_scales, down_scales = (
        lax.all_gather(scale_mixout, "fs", axis=1, tiled=True),
        lax.all_gather(scale_down, "fs", axis=1, tiled=True),
    )
    mixout_bf = w_mixout.astype(jnp.bfloat16)
    mixed_all = lax.all_gather(mixed_out, "tp", axis=1, tiled=True)
    mixout_cols = lax.all_gather(mixout_bf, "fs", axis=1, tiled=True)
    mixout_all = lax.all_gather(mixout_cols, "tp", axis=0, tiled=True)
    mix_term = jnp.dot(mixed_all, mixout_all, preferred_element_type=jnp.float32) * mixout_scales
    residual_rows = (full_rows.astype(jnp.float32) + mix_term).astype(jnp.bfloat16)
    feature_count = tokens.shape[1]
    residual = lax.dynamic_slice_in_dim(
        residual_rows, lax.axis_index("tp") * feature_count, feature_count, 1
    )
    normed_ffn = rms_scaled(residual_rows, ffn_gain)
    gate_proj = add_rows(
        normed_ffn, lax.all_gather(w_gate.astype(jnp.bfloat16), "fs", axis=0, tiled=True)
    )
    up_proj = add_rows(
        normed_ffn, lax.all_gather(w_upward.astype(jnp.bfloat16), "fs", axis=0, tiled=True)
    )
    hidden = (jax.nn.silu(gate_proj * scale_gate) * (up_proj * scale_upward)).astype(jnp.bfloat16)
    down_terms = (
        jnp.dot(
            hidden,
            lax.all_gather(w_down.astype(jnp.bfloat16), "fs", axis=1, tiled=True),
            preferred_element_type=jnp.float32,
        )
        * down_scales
    )
    ffn_share = lax.psum_scatter(
        down_terms.astype(jnp.bfloat16), "tp", scatter_dimension=1, tiled=True
    ).astype(jnp.float32)
    return (residual.astype(jnp.float32) + ffn_share).astype(jnp.bfloat16)


def solution(mesh):
    in_specs = (
        P("fs", "tp"),
        P(),
        P(),
        P("fs", "tp"),
        P("fs", "tp"),
        P("fs", "tp"),
        P(None, "tp"),
        P(None, "tp"),
        P(None, "tp"),
        P(None, "tp"),
        P("tp", "fs"),
        P(None, "fs"),
        P("fs", "tp"),
        P("fs", "tp"),
        P(None, "tp"),
        P(None, "tp"),
        P("tp", "fs"),
        P(None, "fs"),
    )
    out_specs = P("fs", "tp")
    chosen = fused_device if (mesh.shape["fs"], mesh.shape["tp"]) == (8, 4) else plain_device
    return jax.shard_map(
        chosen, mesh=mesh, in_specs=in_specs, out_specs=out_specs, check_vma=False
    )
```

time: 380 us -> 250 us (0.66)
  Pallas kernels: 305 us -> 237 us
  waiting for transfers between devices: 46.7 us -> 0 us
  between operations: 13.4 us -> 0.27 us
  local copies, waits for them, and re-layouts: 0.04 us -> 5.74 us
  other arithmetic: 12 us -> 7.15 us
    pallas_call x1, Pallas kernels: 305 us -> 237 us  [fused_device(): pl.pallas_call(block_kernel, out_shape=jax.ShapeDtypeStruct((count, feat)...]
    reduce_scatter x1 -> x0, waiting for transfers between devices: 46.7 us -> none  [fused_device(): share = lax.psum_scatter(terms, 'tp', scatter_dimension=1, tiled=True)]
    unnamed x18 -> x27, local copies, waits for them, and re-layouts: 0.04 us -> 4.21 us
  transfers between devices with their start and end apart: 1 -> 0, of which waited for: 1 -> 0; matrix products, arithmetic and copies ran while one was open for 0% -> 0% of each run, Pallas kernels for 0% -> 0%
where the time goes in v1:
time: 250 us
  Pallas kernels  237 us (95%)
  other arithmetic  7.15 us (3%)
  local copies, waits for them, and re-layouts  5.74 us (2%)
    pallas_call x1, Pallas kernels, fused_device(): pl.pallas_call(block_kernel, out_shape=jax.ShapeDtypeStruct((count, feat)...  237 us

profile of v1, /device:TPU:3, one launch (start us, length us, event | category | flops | bytes accessed | tf_op | source)
XLA Modules:
  0.0 249.8 jit_solution(11171438625283133600)
XLA Ops:
  0.0 1.4 convert_element_type.16
  1.5 0.0 copy-start
  1.5 0.9 pad_maximum_fusion.1.h_back
  2.5 0.6 copy-done
  3.1 0.0 copy-start.1
  3.1 0.1 convert_element_type.14
  3.2 1.2 copy-done.1
  4.5 0.1 convert_element_type.15
  4.6 0.3 concatenate.34
  4.9 0.2 slice.73
  5.1 0.1 slice.72
  5.2 0.5 concatenate.35
  5.7 0.0 copy-start.2
  5.7 0.0 copy-start.3
  5.7 0.0 copy-start.4
  5.8 1.3 pad_maximum_fusion.h_gated
  7.0 0.0 copy-done.2
  7.0 0.0 copy-start.5
  7.0 0.0 slice-start
  7.0 0.0 slice-start.2
  7.0 0.0 slice-start.3
  7.0 0.0 copy-start.7
  7.1 0.0 copy-start.6
  7.1 0.0 slice-start.1
  7.1 0.0 copy-start.8
  7.1 0.0 copy-start.9
  7.1 0.0 copy-start.10
  7.1 0.0 copy-start.11
  7.1 0.0 copy-start.12
  7.2 0.0 copy-done.3
  7.2 0.0 copy-done.4
  7.2 0.8 pad_maximum_fusion.2.h_mixer
  8.0 0.0 copy-done.5
  8.0 0.7 convert_element_type.13.h_mixout
  8.7 0.0 slice-done
  8.7 0.0 slice-done.2
  8.7 0.0 slice-done.3
  8.7 0.1 concatenate.30
  8.8 0.0 copy-done.7
  8.8 0.1 slice.58
  8.9 0.0 copy-done.6
  8.9 0.1 slice.57
  8.9 0.0 slice-done.1
  8.9 0.1 concatenate.31
  9.0 0.6 maximum_bitcast_fusion.1.s_gated
  9.7 0.0 copy-done.8
  9.7 0.0 copy-done.9
  9.7 0.6 pad_maximum_fusion.3.h_scales
  10.3 0.0 copy-done.10
  10.3 0.0 copy-done.11
  10.3 0.0 copy-done.12
  10.3 0.6 pad_maximum_fusion.4.s_mixer
  10.9 236.7 %shard_map.172 = bf16[1024,512]{1,0:T(8,128)(2,1)} custom-call(bf16[1024,512]{1,0:T(8,128)(2,1)} %tokens.1, f32[1,2048]{1,0:T(1,128)} %bitcast.18, f32[1,2048]{1,0:T(1,128)} %bitcast.19, f32[1,768]{1,0:T(1,128)} %pad_maximum_fusion.4.s_mixer, f32[3,256]{1,0:T(4,128)} %taps.1, f32[2,1408]{1,0:T(2,128)} %maximum_bitcast_fusion.1.s_gated, ...), custom_call_target="tpu_custom_call" | custom-call | tf_op jit(solution)/shard_map/pallas_call | solution.py:570
  247.5 2.3 copy.20
  (12 shorter events, 0.2 us)
Async XLA Ops:
  1.5 1.6 copy-start
  3.1 1.4 copy-start.1
  5.7 1.3 copy-start.2
  5.7 1.4 copy-start.3
  5.7 1.4 copy-start.4
  7.0 1.0 copy-start.5
  7.0 1.7 slice-start
  7.0 1.7 slice-start.2
  7.0 1.7 slice-start.3
  7.0 1.7 copy-start.7
  7.1 1.8 copy-start.6
  7.1 1.9 slice-start.1
  7.1 2.6 %copy-start.8 = (f32[1,256]{1,0:T(1,128)S(1)}, f32[1,256]{1,0:T(1,128)}, u32[]{:S(2)}) copy-start(f32[1,256]{1,0:T(1,128)} %param.29) | copy-start | bytes 3076
  7.1 2.6 %copy-start.9 = (f32[1,256]{1,0:T(1,128)S(1)}, f32[1,256]{1,0:T(1,128)}, u32[]{:S(2)}) copy-start(f32[1,256]{1,0:T(1,128)} %param.35) | copy-start | bytes 3076
  7.1 3.2 %copy-start.10 = (f32[1,256]{1,0:T(1,128)S(1)}, f32[1,256]{1,0:T(1,128)}, u32[]{:S(2)}) copy-start(f32[1,256]{1,0:T(1,128)} %param.26) | copy-start | bytes 3076
  7.1 3.2 %copy-start.11 = (f32[1,256]{1,0:T(1,128)S(1)}, f32[1,256]{1,0:T(1,128)}, u32[]{:S(2)}) copy-start(f32[1,256]{1,0:T(1,128)} %param.25) | copy-start | bytes 3076
  7.1 3.2 %copy-start.12 = (f32[1,256]{1,0:T(1,128)S(1)}, f32[1,256]{1,0:T(1,128)}, u32[]{:S(2)}) copy-start(f32[1,256]{1,0:T(1,128)} %param.24) | copy-start | bytes 3076

commit v2 on v1

--- a/solution.py
+++ b/solution.py
@@ -36,9 +36,10 @@
 
 
 def block_kernel(
-    tokens, mixer_gain, ffn_gain, s_mixer, taps, s_gated,
-    h_scales, h_mixer, h_mixout, h_gated, h_back,
+    tokens, mixer_gain, ffn_gain, w_outer, w_inner, w_value, s_outer, s_inner, s_value, taps,
+    w_mixout, s_mixout, w_gate, w_upward, s_gate, s_upward, w_down, s_down,
     out,
+    h_scales, h_mixer, h_mixout, h_gated, h_back, s_gated, raw_gate, raw_up, raw_down,
     act, mixer, mixout, gated, back, scales, mixed, hidden, residual_own,
     part, from_core, from_y, from_x,
     z_send, y_send, fs_recv, tp_send, tp_recv, mx_send, mx_recv,
@@ -58,12 +59,24 @@
     sibling = ex * 2 + (1 - core)
     across = (1 - ex) * 2 + core
 
+    def fetch(k):
+        source, target = ((w_gate, raw_gate), (w_upward, raw_up), (w_down, raw_down))[k]
+        return pltpu.make_async_copy(source, target, local_sem.at[6 + k])
+
+    for k in range(3):
+        fetch(k).start()
     barrier = pltpu.get_barrier_semaphore()
     ring = [lax.rem(zed + step, DEPTH) * WIDTH + why for step in (1, DEPTH - 1)]
     for peer in (beside, *ring):
         pl.semaphore_signal(barrier, inc=1, device_id={"fs": peer}, device_id_type=MESH)
     for peer in (sibling, across):
         pl.semaphore_signal(barrier, inc=1, device_id={"tp": peer}, device_id_type=MESH)
+    wide = w_outer.shape[1]
+    for k, w in enumerate((w_outer, w_inner, w_value)):
+        h_mixer[:, k * wide : (k + 1) * wide] = w[...].astype(bf16)
+    h_mixout[...] = w_mixout[...].astype(bf16)
+    for k, row in enumerate((s_mixout, s_down)):
+        h_scales[k * 8 : (k + 1) * 8, :] = jnp.broadcast_to(row[...], (8, row.shape[1]))
     pl.semaphore_wait(barrier, 5)
 
     fulls = (scales, mixer, mixout, gated, back)
@@ -230,9 +243,40 @@
     tp_first(0)
     mx_first(me, h_mixout)
     own_tokens.start()
-    for p in range(5):
+    for p in firsts:
         own(p).start()
     units = h_back.shape[1]
+    main = units // 128 * 128
+    middle, after = pl.ds(main, 128), main + 128
+
+    def share_out(gate, up, write):
+        write(0, pl.ds(0, main), gate[:, :main])
+        write(0, pl.ds(after, main), up[:, :main])
+        write(1, pl.ds(0, main), gate[:, after:])
+        write(1, pl.ds(after, main), up[:, after:])
+        gate, up = gate[:, middle], up[:, middle]
+        low = lax.broadcasted_iota(jnp.int32, gate.shape, 1) < 64
+        write(0, middle, jnp.where(low, gate, pltpu.roll(up, 64, 1)))
+        write(1, middle, jnp.where(low, pltpu.roll(gate, 64, 1), up))
+
+    def write_scale(half, lanes, values):
+        s_gated[half : half + 1, lanes] = values
+
+    def write_gated(half, lanes, values):
+        h_gated[half, :, lanes] = values.astype(bf16)
+
+    for k in range(3):
+        fetch(k).wait()
+    share_out(raw_gate, raw_up, write_gated)
+    h_back[0] = raw_down[:units, :].astype(bf16)
+    h_back[1, :main, :] = raw_down[after:, :].astype(bf16)
+    h_back[1, main:, :] = raw_down[units:after, :].astype(bf16)
+    spread = [jnp.broadcast_to(row[...], (8, row.shape[1])) for row in (s_gate, s_upward)]
+    share_out(
+        *spread, lambda half, lanes, values: write_scale(half, lanes, values[0:1])
+    )
+    for p in (GATED, BACK):
+        own(p).start()
     back[units:, :] = jnp.zeros((back.shape[0] - units, back.shape[1]), bf16)
 
     relay_first(1)
@@ -265,8 +309,8 @@
     @pl.loop(0, tiles)
     def _(i):
         normed = normalised(act[own_rows(i), :].astype(f32), mixer_gain)
-        three = jnp.dot(normed, mixer[...], preferred_element_type=f32) * s_mixer[...]
-        product = three[:, chan : 2 * chan] * three[:, 2 * chan :]
+        three = jnp.dot(normed, mixer[...], preferred_element_type=f32)
+        product = (three[:, chan : 2 * chan] * s_inner[...]) * (three[:, 2 * chan :] * s_value[...])
         row = lax.rem(lax.broadcasted_iota(jnp.int32, product.shape, 0), SEQ_LEN)
         total = jnp.zeros_like(product)
         last = taps.shape[0] - 1
@@ -277,7 +321,7 @@
                 moved = jnp.where(row >= gap, pltpu.roll(product, gap, 0), 0.0)
             total = total + taps[j : j + 1, :] * moved
         mixed[tile(i), pl.ds(pl.multiple_of(tp * chan, chan), chan)] = (
-            three[:, :chan] * total
+            three[:, :chan] * s_outer[...] * total
         ).astype(bf16)
 
     tp_first(1)
@@ -325,13 +369,11 @@
         act[own_rows(i), :] = normalised(residual.astype(f32), ffn_gain)
         pl.when(step < share)(lambda: act_copy(why, core, step, 0).start())
 
-    z_own(BACK, why, own_src[BACK])
+    relay(GATED, 2, other)
     arrived(BACK, beside)
-    z_own(BACK, other, None)
-    relay(GATED, 2, other)
-    for row in (why, other):
-        for s in (1, 2):
-            relay(BACK, s, row)
+    own(BACK).wait()
+    for row in range(WIDTH):
+        z_own(BACK, row, None)
     for q in range(share):
         act_copy(other, core, q, 0).wait_recv()
         act_copy(other, core, q, 1).start()
@@ -339,8 +381,6 @@
     for row in (why, other):
         for s in (1, 2, 3):
             settle(GATED, s, row)
-
-    main = (gated.shape[1] // 256) * 128
 
     def activate(first, steps):
         @pl.loop(0, steps)
@@ -356,12 +396,6 @@
             lane = lax.broadcasted_iota(jnp.int32, rest.shape, 1)
             hidden[rows, main:] = jnp.where(lane < 64, rest, 0.0).astype(bf16)
 
-    activate(base, tiles)
-    for q in range(share):
-        act_copy(other, 1 - core, q, 1).wait_recv()
-    activate(other * count, tiles)
-
-    own(BACK).wait()
     pieces = count // PIECE
 
     def piece(t):
@@ -370,70 +404,68 @@
     def block_at(k):
         return lax.rem(zed + k * (1 - 2 * lax.div(zed, last_z)) + DEPTH, DEPTH)
 
-    def core_copy(j, t):
+    def core_copy(j, row, t):
         line = lax.div(j, 2)
         return pltpu.make_async_remote_copy(
-            src_ref=part.at[j, piece(t), :],
-            dst_ref=from_core.at[line, piece(t), :],
-            send_sem=core_send.at[line, t],
-            recv_sem=core_recv.at[line, t],
+            src_ref=part.at[j, row, piece(t), :],
+            dst_ref=from_core.at[line, row, piece(t), :],
+            send_sem=core_send.at[line, row, t],
+            recv_sem=core_recv.at[line, row, t],
             device_id={"tp": sibling},
             device_id_type=MESH,
         )
 
-    def sum_copy(j, q):
+    def sum_copy(j, row, q):
         line = lax.div(j, 2)
         return pltpu.make_async_remote_copy(
-            src_ref=part.at[j, piece(other * pieces + q), :],
-            dst_ref=from_y.at[line, piece(q), :],
-            send_sem=sum_send.at[line, q],
-            recv_sem=sum_recv.at[line, q],
+            src_ref=part.at[j, row, piece(other * pieces + q), :],
+            dst_ref=from_y.at[line, row, piece(q), :],
+            send_sem=sum_send.at[line, row, q],
+            recv_sem=sum_recv.at[line, row, q],
             device_id={"fs": beside},
             device_id_type=MESH,
         )
 
-    def last_copy(j, q):
+    def last_copy(j, row, q):
         return pltpu.make_async_remote_copy(
-            src_ref=part.at[j, piece(why * pieces + q), :],
-            dst_ref=from_x.at[piece(q), :],
-            send_sem=last_send.at[q],
-            recv_sem=last_recv.at[q],
+            src_ref=part.at[j, row, piece(why * pieces + q), :],
+            dst_ref=from_x.at[row, piece(q), :],
+            send_sem=last_send.at[row, q],
+            recv_sem=last_recv.at[row, q],
             device_id={"tp": across},
             device_id_type=MESH,
         )
 
-    def multiply(k):
+    def multiply(k, row, half):
         j = block_at(k)
-        if k:
-            for row in range(WIDTH):
-                pl.when(outer)(lambda: arrived(BACK, j * WIDTH + row))
-        columns = pl.ds(pl.multiple_of(j * feat, feat), feat)
-
-        @pl.loop(0, WIDTH * pieces)
-        def _(step):
-            t = lax.rem(step + other * pieces, WIDTH * pieces)
+        wide = h_back.shape[2]
+        columns = pl.ds(pl.multiple_of((j * WIDTH + row) * wide, wide), wide)
+
+        @pl.loop(0, pieces)
+        def _(q):
+            t = half * pieces + q
             term = jnp.dot(hidden[piece(t), :], back[:, columns], preferred_element_type=f32)
-            part[j, piece(t), :] = (term * scales[8:9, columns]).astype(bf16)
-            pl.when(core != lax.rem(j, 2))(lambda: core_copy(j, t).start())
-
-    def added(j, t, extra):
-        return part[j, piece(t), :].astype(f32) + extra.astype(f32)
-
-    def reduce_core(k):
+            part[j, row, piece(t), :] = (term * scales[8:9, columns]).astype(bf16)
+            pl.when(core != lax.rem(j, 2))(lambda: core_copy(j, row, t).start())
+
+    def added(j, row, t, extra):
+        return part[j, row, piece(t), :].astype(f32) + extra.astype(f32)
+
+    def reduce_core(k, row, half):
         j = block_at(k)
 
         @pl.when(core == lax.rem(j, 2))
         def _():
             line = lax.div(j, 2)
-            for half in (other, why):
-                for q in range(pieces):
-                    t = half * pieces + q
-                    core_copy(j, t).wait_recv()
-                    part[j, piece(t), :] = added(j, t, from_core[line, piece(t), :]).astype(bf16)
-                    if half is other:
-                        sum_copy(j, q).start()
-
-    def reduce_y(k):
+            for q in range(pieces):
+                t = half * pieces + q
+                core_copy(j, row, t).wait_recv()
+                total = added(j, row, t, from_core[line, row, piece(t), :])
+                part[j, row, piece(t), :] = total.astype(bf16)
+                if half is other:
+                    sum_copy(j, row, q).start()
+
+    def reduce_y(k, row):
         j = block_at(k)
 
         @pl.when(core == lax.rem(j, 2))
@@ -441,31 +473,55 @@
             line = lax.div(j, 2)
             for q in range(pieces):
                 t = why * pieces + q
-                sum_copy(j, q).wait_recv()
-                part[j, piece(t), :] = added(j, t, from_y[line, piece(q), :]).astype(bf16)
-                pl.when(ex != line)(lambda: last_copy(j, q).start())
-
-    def reduce_x(k):
+                sum_copy(j, row, q).wait_recv()
+                total = added(j, row, t, from_y[line, row, piece(q), :])
+                part[j, row, piece(t), :] = total.astype(bf16)
+                pl.when(ex != line)(lambda: last_copy(j, row, q).start())
+
+    def reduce_x(k, row):
         j = block_at(k)
+        wide = h_back.shape[2]
 
         @pl.when(tp == j)
         def _():
+            columns = pl.ds(row * wide, wide)
             for q in range(pieces):
                 t = why * pieces + q
-                last_copy(j, q).wait_recv()
-                total = added(j, t, from_x[piece(q), :])
-                out[piece(q), :] = (residual_own[piece(q), :].astype(f32) + total).astype(bf16)
-
-    for k in range(DEPTH):
-        multiply(k)
-        reduce_core(k)
-        if k > 0:
-            reduce_y(k - 1)
-        if k > 1:
-            reduce_x(k - 2)
-    reduce_y(DEPTH - 1)
-    reduce_x(DEPTH - 2)
-    reduce_x(DEPTH - 1)
+                last_copy(j, row, q).wait_recv()
+                total = added(j, row, t, from_x[row, piece(q), :])
+                kept = residual_own[piece(q), columns].astype(f32)
+                out[piece(q), columns] = (kept + total).astype(bf16)
+
+    for q in range(share):
+        act_copy(other, 1 - core, q, 1).wait_recv()
+    activate(other * count, tiles)
+    for row in range(WIDTH):
+        relay(BACK, 1, row)
+    for row in range(WIDTH):
+        multiply(0, row, other)
+        reduce_core(0, row, other)
+    activate(base, tiles)
+    for row in range(WIDTH):
+        relay(BACK, 2, row)
+    for row in range(WIDTH):
+        multiply(0, row, why)
+        reduce_core(0, row, why)
+
+    order = [(k, row) for k in range(DEPTH) for row in range(WIDTH)]
+    for u, (k, row) in enumerate(order):
+        if k:
+            owner = block_at(k) * WIDTH + row
+            pl.when(outer)(lambda: arrived(BACK, owner))
+            for half in (other, why):
+                multiply(k, row, half)
+                reduce_core(k, row, half)
+            if u == WIDTH:
+                reduce_y(*order[0])
+            reduce_y(*order[u - 1])
+            reduce_x(*order[u - 2])
+    reduce_y(*order[-1])
+    reduce_x(*order[-2])
+    reduce_x(*order[-1])
 
     def sent(p, row):
         owner = zed * WIDTH + row
@@ -495,33 +551,18 @@
         act_copy(why, core, q, 0).wait_send()
         act_copy(other, core, q, 1).wait_send()
     for j in range(DEPTH):
-
-        @pl.when(core != j % 2)
-        def _():
-            for t in range(WIDTH * pieces):
-                core_copy(j, t).wait_send()
-
-        @pl.when(core == j % 2)
-        def _():
-            for q in range(pieces):
-                sum_copy(j, q).wait_send()
-                pl.when(ex != j // 2)(lambda: last_copy(j, q).wait_send())
-
-
-def halves(gate, up, axis_units):
-    half = axis_units // 2
-    main = half // 128 * 128
-    end = axis_units - main
-    return jnp.stack(
-        [
-            jnp.concatenate(
-                [gate[:, :main], gate[:, main:half], up[:, main:half], up[:, :main]], axis=1
-            ),
-            jnp.concatenate(
-                [gate[:, end:], gate[:, half:end], up[:, half:end], up[:, end:]], axis=1
-            ),
-        ]
-    )
+        for row in range(WIDTH):
+
+            @pl.when(core != j % 2)
+            def _():
+                for t in range(WIDTH * pieces):
+                    core_copy(j, row, t).wait_send()
+
+            @pl.when(core == j % 2)
+            def _():
+                for q in range(pieces):
+                    sum_copy(j, row, q).wait_send()
+                    pl.when(ex != j // 2)(lambda: last_copy(j, row, q).wait_send())
 
 
 def fused_device(
@@ -551,28 +592,26 @@
     units = w_gate.shape[1]
     cols = w_down.shape[1]
     half = units // 2
-    main = half // 128 * 128
-    padded = main + 128
-    shard = jnp.concatenate([w_outer, w_inner, w_value], axis=1).astype(bf16)
-    s_mixer = jnp.concatenate([scale_outer, scale_inner, scale_value], axis=1)
-    scale_shard = jnp.concatenate(
-        [jnp.broadcast_to(scale_mixout, (8, cols)), jnp.broadcast_to(scale_down, (8, cols))], axis=0
-    )
-    h_gated = halves(w_gate.astype(bf16), w_upward.astype(bf16), units)
-    s_gated = halves(scale_gate, scale_upward, units)[:, 0]
-    w_back = w_down.astype(bf16)
-    h_back = jnp.stack(
-        [w_back[:half], jnp.concatenate([w_back[units - main :], w_back[half : units - main]])]
-    )
+    padded = half // 128 * 128 + 128
     vmem = pl.BlockSpec(memory_space=pltpu.VMEM)
+    hbm = pl.BlockSpec(memory_space=pl.ANY)
     dma = pltpu.SemaphoreType.DMA
     owners = DEPTH * WIDTH
     return pl.pallas_call(
         block_kernel,
         out_shape=jax.ShapeDtypeStruct((count, feat), bf16),
-        in_specs=[vmem] * 11,
+        in_specs=[hbm if k in (12, 13, 16) else vmem for k in range(18)],
         out_specs=vmem,
         scratch_shapes=[
+            pltpu.VMEM((16, cols), jnp.float32),
+            pltpu.VMEM((w_outer.shape[0], 3 * chan), bf16),
+            pltpu.VMEM(w_mixout.shape, bf16),
+            pltpu.VMEM((2, w_gate.shape[0], units), bf16),
+            pltpu.VMEM((2, half, cols), bf16),
+            pltpu.VMEM((2, units), jnp.float32),
+            pltpu.VMEM(w_gate.shape, jnp.float32),
+            pltpu.VMEM(w_upward.shape, jnp.float32),
+            pltpu.VMEM(w_down.shape, jnp.float32),
             pltpu.VMEM((WIDTH * count, model), bf16),
             pltpu.VMEM((model, 3 * chan), bf16),
             pltpu.VMEM((TP * chan, model), bf16),
@@ -582,10 +621,10 @@
             pltpu.VMEM((count, TP * chan), bf16),
             pltpu.VMEM((WIDTH * count, padded), bf16),
             pltpu.VMEM((count, feat), bf16),
-            pltpu.VMEM((DEPTH, WIDTH * count, feat), bf16),
-            pltpu.VMEM((2, WIDTH * count, feat), bf16),
-            pltpu.VMEM((2, count, feat), bf16),
-            pltpu.VMEM((count, feat), bf16),
+            pltpu.VMEM((DEPTH, WIDTH, WIDTH * count, cols), bf16),
+            pltpu.VMEM((2, WIDTH, WIDTH * count, cols), bf16),
+            pltpu.VMEM((2, WIDTH, count, cols), bf16),
+            pltpu.VMEM((WIDTH, count, cols), bf16),
             dma((5, owners, 2)),
             dma((5, owners)),
             dma((5, owners)),
@@ -595,20 +634,21 @@
             dma((owners, 3)),
             dma((2, 2)),
             dma((2, 2)),
-            dma((2, 4)),
-            dma((2, 4)),
-            dma((2, 2)),
-            dma((2, 2)),
-            dma((2,)),
-            dma((2,)),
-            dma((6,)),
+            dma((2, WIDTH, 4)),
+            dma((2, WIDTH, 4)),
+            dma((2, WIDTH, 2)),
+            dma((2, WIDTH, 2)),
+            dma((WIDTH, 2)),
+            dma((WIDTH, 2)),
+            dma((9,)),
         ],
         compiler_params=pltpu.CompilerParams(
             collective_id=0, has_side_effects=True, vmem_limit_bytes=62 * 1024 * 1024
         ),
     )(
-        tokens, mixer_gain[None], ffn_gain[None], s_mixer, conv_taps, s_gated,
-        scale_shard, shard, w_mixout.astype(bf16), h_gated, h_back,
+        tokens, mixer_gain[None], ffn_gain[None], w_outer, w_inner, w_value,
+        scale_outer, scale_inner, scale_value, conv_taps, w_mixout, scale_mixout,
+        w_gate, w_upward, scale_gate, scale_upward, w_down, scale_down,
     )
 
 

time: 250 us -> 220 us (0.88)
  Pallas kernels: 237 us -> 216 us
  other arithmetic: 7.15 us -> 0 us
  local copies, waits for them, and re-layouts: 5.74 us -> 2.26 us
    pallas_call x1, Pallas kernels: 237 us -> 216 us  [fused_device(): pl.pallas_call(block_kernel, out_shape=jax.ShapeDtypeStruct((count, feat)...]
where the time goes in v2:
time: 220 us; the launch traced here: 218 us
  Pallas kernels  216 us (98%)
  local copies, waits for them, and re-layouts  2.26 us (1%)
    pallas_call x1, Pallas kernels, fused_device(): pl.pallas_call(block_kernel, out_shape=jax.ShapeDtypeStruct((count, feat)...  216 us

profile of v2, /device:TPU:3, one launch (start us, length us, event | category | flops | bytes accessed | tf_op | source)
XLA Modules:
  0.0 218.4 jit_solution(17122223737201394033)
XLA Ops:
  0.0 216.2 %shard_map.172 = bf16[1024,512]{1,0:T(8,128)(2,1)} custom-call(bf16[1024,512]{1,0:T(8,128)(2,1)} %tokens.1, f32[1,2048]{1,0:T(1,128)} %bitcast.2, f32[1,2048]{1,0:T(1,128)} %bitcast.3, f32[256,256]{1,0:T(8,128)} %w_outer.1, f32[256,256]{1,0:T(8,128)} %w_inner.1, f32[256,256]{1,0:T(8,128)} %w_value.1, f32[1,256]{1,0:T(1,128)} %s_outer.1, f32[1,256]{1,0:T(1,128)} %s_inner.1, ...), custom_call_target="tpu_custom_call" | custom-call | tf_op jit(solution)/shard_map/pallas_call | solution.py:600
  216.2 2.3 %copy.20 = bf16[1024,512]{1,0:T(8,128)(2,1)} copy(bf16[1024,512]{1,0:T(8,128)(2,1)} %shard_map.172) | data formatting | bytes 2097152

commit v3 on v2

--- a/solution.py
+++ b/solution.py
@@ -284,8 +284,7 @@
     relay_first(2)
     z_own(GATED, why, own_src[GATED])
     relay_first(3)
-    for p in (GATED, BACK):
-        y_copy(p, me, (h_gated if p == GATED else h_back).at[other]).start()
+    y_copy(GATED, me, h_gated.at[other]).start()
     for s in range(DEPTH):
         from_beside(s)
     relay(GATED, 1, why)
@@ -341,24 +340,30 @@
         tp_copy(0, k).wait_send()
 
     feat = tokens.shape[1]
-    share = tiles // 2
-
-    def act_copy(half, lead, q, k):
-        spot = act.at[
-            pl.ds(pl.multiple_of(half * count + (lead * share + q) * ROWS, ROWS), ROWS), :
-        ]
+    quarter = count // TP
+    strip = quarter // 2
+
+    def act_copy(k, h):
+        half, owner, target = (
+            (why, tp, {"fs": beside}),
+            (other, tp, {"tp": sibling}),
+            (other, tp, {"tp": across}),
+            (other, across, {"tp": sibling}),
+        )[k]
+        first = half * count + owner * quarter + h * strip
+        spot = act.at[pl.ds(pl.multiple_of(first, strip), strip), :]
         return pltpu.make_async_remote_copy(
             src_ref=spot,
             dst_ref=spot,
-            send_sem=act_send.at[q, k],
-            recv_sem=act_recv.at[q, k],
-            device_id={"fs": beside} if k == 0 else {"tp": sibling},
+            send_sem=act_send.at[k, h],
+            recv_sem=act_recv.at[k, h],
+            device_id=target,
             device_id_type=MESH,
         )
 
     @pl.loop(0, tiles)
     def _(step):
-        i = lax.rem(step + core * share, tiles)
+        i = lax.rem(step + tp, tiles)
         term = jnp.dot(mixed[tile(i), :], mixout[...], preferred_element_type=f32)
         term = term * scales[0:1, :]
         residual = (act[own_rows(i), :].astype(f32) + term).astype(bf16)
@@ -367,16 +372,29 @@
             own_rows(i), pl.ds(pl.multiple_of(tp * feat, feat), feat)
         ]
         act[own_rows(i), :] = normalised(residual.astype(f32), ffn_gain)
-        pl.when(step < share)(lambda: act_copy(why, core, step, 0).start())
-
+
+        @pl.when(step == 0)
+        def _():
+            for h in range(2):
+                act_copy(0, h).start()
+
+    y_copy(BACK, me, h_back.at[other]).start()
+
+    def spread_act(h):
+        act_copy(0, h).wait_recv()
+        act_copy(2, h).start()
+        act_copy(1, h).start()
+
+    spread_act(0)
     relay(GATED, 2, other)
+    spread_act(1)
     arrived(BACK, beside)
     own(BACK).wait()
     for row in range(WIDTH):
         z_own(BACK, row, None)
-    for q in range(share):
-        act_copy(other, core, q, 0).wait_recv()
-        act_copy(other, core, q, 1).start()
+    for h in range(2):
+        act_copy(2, h).wait_recv()
+        act_copy(3, h).start()
     own(GATED).wait()
     for row in (why, other):
         for s in (1, 2, 3):
@@ -426,15 +444,18 @@
             device_id_type=MESH,
         )
 
-    def last_copy(j, row, q):
+    def last_copy(j, row, t):
         return pltpu.make_async_remote_copy(
-            src_ref=part.at[j, row, piece(why * pieces + q), :],
-            dst_ref=from_x.at[row, piece(q), :],
-            send_sem=last_send.at[row, q],
-            recv_sem=last_recv.at[row, q],
+            src_ref=part.at[j, row, piece(t), :],
+            dst_ref=from_x.at[row, piece(t), :],
+            send_sem=last_send.at[row, t],
+            recv_sem=last_recv.at[row, t],
             device_id={"tp": across},
             device_id_type=MESH,
         )
+
+    def x_first(k, row):
+        return row == 0 and k < last_z
 
     def multiply(k, row, half):
         j = block_at(k)
@@ -451,7 +472,7 @@
     def added(j, row, t, extra):
         return part[j, row, piece(t), :].astype(f32) + extra.astype(f32)
 
-    def reduce_core(k, row, half):
+    def stage_1(k, row, half):
         j = block_at(k)
 
         @pl.when(core == lax.rem(j, 2))
@@ -462,23 +483,40 @@
                 core_copy(j, row, t).wait_recv()
                 total = added(j, row, t, from_core[line, row, piece(t), :])
                 part[j, row, piece(t), :] = total.astype(bf16)
-                if half is other:
+                if x_first(k, row):
+                    pl.when(ex != line)(lambda: last_copy(j, row, t).start())
+                elif half is other:
                     sum_copy(j, row, q).start()
 
-    def reduce_y(k, row):
+    def stage_2(k, row):
         j = block_at(k)
-
-        @pl.when(core == lax.rem(j, 2))
-        def _():
-            line = lax.div(j, 2)
+        line = lax.div(j, 2)
+        mine = core == lax.rem(j, 2)
+
+        def x_sums():
+            for half in (other, why):
+                for q in range(pieces):
+                    t = half * pieces + q
+                    last_copy(j, row, t).wait_recv()
+                    total = added(j, row, t, from_x[row, piece(t), :])
+                    part[j, row, piece(t), :] = total.astype(bf16)
+                    if half is other:
+                        sum_copy(j, row, q).start()
+
+        def y_sums():
             for q in range(pieces):
                 t = why * pieces + q
                 sum_copy(j, row, q).wait_recv()
                 total = added(j, row, t, from_y[line, row, piece(q), :])
                 part[j, row, piece(t), :] = total.astype(bf16)
-                pl.when(ex != line)(lambda: last_copy(j, row, q).start())
-
-    def reduce_x(k, row):
+                pl.when(ex != line)(lambda: last_copy(j, row, t).start())
+
+        if x_first(k, row):
+            pl.when(mine & (ex == line))(x_sums)
+        else:
+            pl.when(mine)(y_sums)
+
+    def stage_3(k, row):
         j = block_at(k)
         wide = h_back.shape[2]
 
@@ -487,41 +525,51 @@
             columns = pl.ds(row * wide, wide)
             for q in range(pieces):
                 t = why * pieces + q
-                last_copy(j, row, q).wait_recv()
-                total = added(j, row, t, from_x[row, piece(q), :])
+                if x_first(k, row):
+                    sum_copy(j, row, q).wait_recv()
+                    extra = from_y[lax.div(j, 2), row, piece(q), :]
+                else:
+                    last_copy(j, row, t).wait_recv()
+                    extra = from_x[row, piece(t), :]
                 kept = residual_own[piece(q), columns].astype(f32)
-                out[piece(q), columns] = (kept + total).astype(bf16)
-
-    for q in range(share):
-        act_copy(other, 1 - core, q, 1).wait_recv()
+                out[piece(q), columns] = (kept + added(j, row, t, extra)).astype(bf16)
+
+    for h in range(2):
+        act_copy(1, h).wait_recv()
+        act_copy(3, h).wait_recv()
     activate(other * count, tiles)
     for row in range(WIDTH):
         relay(BACK, 1, row)
     for row in range(WIDTH):
         multiply(0, row, other)
-        reduce_core(0, row, other)
+        stage_1(0, row, other)
     activate(base, tiles)
     for row in range(WIDTH):
         relay(BACK, 2, row)
     for row in range(WIDTH):
         multiply(0, row, why)
-        reduce_core(0, row, why)
+        stage_1(0, row, why)
 
     order = [(k, row) for k in range(DEPTH) for row in range(WIDTH)]
+    after_unit = {
+        3: ((stage_2, 1), (stage_2, 0)),
+        4: ((stage_2, 3),),
+        5: ((stage_2, 2), (stage_3, 1), (stage_3, 0)),
+        6: ((stage_2, 5), (stage_2, 4), (stage_3, 3)),
+        7: (
+            (stage_2, 6), (stage_3, 2), (stage_2, 7), (stage_3, 5), (stage_3, 4), (stage_3, 6),
+            (stage_3, 7),
+        ),
+    }
     for u, (k, row) in enumerate(order):
         if k:
             owner = block_at(k) * WIDTH + row
             pl.when(outer)(lambda: arrived(BACK, owner))
             for half in (other, why):
                 multiply(k, row, half)
-                reduce_core(k, row, half)
-            if u == WIDTH:
-                reduce_y(*order[0])
-            reduce_y(*order[u - 1])
-            reduce_x(*order[u - 2])
-    reduce_y(*order[-1])
-    reduce_x(*order[-2])
-    reduce_x(*order[-1])
+                stage_1(k, row, half)
+        for stage, unit in after_unit.get(u, ()):
+            stage(*order[unit])
 
     def sent(p, row):
         owner = zed * WIDTH + row
@@ -547,22 +595,31 @@
             mx_copy(owner, k).wait_send()
     for k in range(3):
         tp_copy(1, k).wait_send()
-    for q in range(share):
-        act_copy(why, core, q, 0).wait_send()
-        act_copy(other, core, q, 1).wait_send()
-    for j in range(DEPTH):
-        for row in range(WIDTH):
-
-            @pl.when(core != j % 2)
-            def _():
-                for t in range(WIDTH * pieces):
-                    core_copy(j, row, t).wait_send()
-
-            @pl.when(core == j % 2)
-            def _():
+    for k in range(4):
+        for h in range(2):
+            act_copy(k, h).wait_send()
+    for k, row in order:
+        j = block_at(k)
+        line = lax.div(j, 2)
+        mine = core == lax.rem(j, 2)
+
+        @pl.when(core != lax.rem(j, 2))
+        def _():
+            for t in range(WIDTH * pieces):
+                core_copy(j, row, t).wait_send()
+
+        def sums_sent():
+            for q in range(pieces):
+                sum_copy(j, row, q).wait_send()
+
+        def lasts_sent(halves):
+            for half in halves:
                 for q in range(pieces):
-                    sum_copy(j, row, q).wait_send()
-                    pl.when(ex != j // 2)(lambda: last_copy(j, row, q).wait_send())
+                    last_copy(j, row, half * pieces + q).wait_send()
+
+        first = x_first(k, row)
+        pl.when(mine & (ex == line) if first else mine)(sums_sent)
+        pl.when(mine & (ex != line))(lambda: lasts_sent((other, why) if first else (why,)))
 
 
 def fused_device(
@@ -624,7 +681,7 @@
             pltpu.VMEM((DEPTH, WIDTH, WIDTH * count, cols), bf16),
             pltpu.VMEM((2, WIDTH, WIDTH * count, cols), bf16),
             pltpu.VMEM((2, WIDTH, count, cols), bf16),
-            pltpu.VMEM((WIDTH, count, cols), bf16),
+            pltpu.VMEM((WIDTH, WIDTH * count, cols), bf16),
             dma((5, owners, 2)),
             dma((5, owners)),
             dma((5, owners)),
@@ -632,14 +689,14 @@
             dma((2, 3)),
             dma((owners, 3)),
             dma((owners, 3)),
-            dma((2, 2)),
-            dma((2, 2)),
+            dma((4, 2)),
+            dma((4, 2)),
             dma((2, WIDTH, 4)),
             dma((2, WIDTH, 4)),
             dma((2, WIDTH, 2)),
             dma((2, WIDTH, 2)),
-            dma((WIDTH, 2)),
-            dma((WIDTH, 2)),
+            dma((WIDTH, 4)),
+            dma((WIDTH, 4)),
             dma((9,)),
         ],
         compiler_params=pltpu.CompilerParams(

time: 220 us -> 210 us (0.955)
  Pallas kernels: 216 us -> 208 us
    pallas_call x1, Pallas kernels: 216 us -> 208 us  [fused_device(): pl.pallas_call(block_kernel, out_shape=jax.ShapeDtypeStruct((count, feat)...]
where the time goes in v3:
time: 210 us
  Pallas kernels  208 us (99%)
  local copies, waits for them, and re-layouts  2.26 us (1%)
    pallas_call x1, Pallas kernels, fused_device(): pl.pallas_call(block_kernel, out_shape=jax.ShapeDtypeStruct((count, feat)...  208 us

profile of v3, /device:TPU:3, one launch (start us, length us, event | category | flops | bytes accessed | tf_op | source)
XLA Modules:
  0.0 210.1 jit_solution(17496809289047375339)
XLA Ops:
  0.0 207.8 %shard_map.172 = bf16[1024,512]{1,0:T(8,128)(2,1)} custom-call(bf16[1024,512]{1,0:T(8,128)(2,1)} %tokens.1, f32[1,2048]{1,0:T(1,128)} %bitcast.2, f32[1,2048]{1,0:T(1,128)} %bitcast.3, f32[256,256]{1,0:T(8,128)} %w_outer.1, f32[256,256]{1,0:T(8,128)} %w_inner.1, f32[256,256]{1,0:T(8,128)} %w_value.1, f32[1,256]{1,0:T(1,128)} %s_outer.1, f32[1,256]{1,0:T(1,128)} %s_inner.1, ...), custom_call_target="tpu_custom_call" | custom-call | tf_op jit(solution)/shard_map/pallas_call | solution.py:657
  207.8 2.3 %copy.20 = bf16[1024,512]{1,0:T(8,128)(2,1)} copy(bf16[1024,512]{1,0:T(8,128)(2,1)} %shard_map.172) | data formatting | bytes 2097152

commit v4 on v3

--- a/solution.py
+++ b/solution.py
@@ -31,7 +31,7 @@
 ROWS = 256
 PIECE = 512
 UP, DOWN = 0, 1
-SCALES, MIXER, MIXOUT, GATED, BACK = range(5)
+SCALES, MIXER, MIXOUT, LEAD, REST, BACK = range(6)
 MESH = pl.DeviceIdType.MESH
 
 
@@ -39,10 +39,11 @@
     tokens, mixer_gain, ffn_gain, w_outer, w_inner, w_value, s_outer, s_inner, s_value, taps,
     w_mixout, s_mixout, w_gate, w_upward, s_gate, s_upward, w_down, s_down,
     out,
-    h_scales, h_mixer, h_mixout, h_gated, h_back, s_gated, raw_gate, raw_up, raw_down,
-    act, mixer, mixout, gated, back, scales, mixed, hidden, residual_own,
+    h_scales, h_mixer, h_mixout, h_lead, h_rest, h_back, s_lead, s_rest, raw_gate, raw_up, raw_down,
+    raw_mixer, raw_mixout, raw_scale,
+    act, mixer, mixout, lead, rest, back, scales, mixed, hidden, residual_own,
     part, from_core, from_y, from_x,
-    z_send, y_send, fs_recv, tp_send, tp_recv, mx_send, mx_recv,
+    z_send, y_send, fs_recv, tp_send, tp_recv, mx_send, mx_recv, mx_whole,
     act_send, act_recv, core_send, core_recv, sum_send, sum_recv, last_send, last_recv,
     local_sem,
 ):
@@ -59,11 +60,16 @@
     sibling = ex * 2 + (1 - core)
     across = (1 - ex) * 2 + core
 
+    wide = w_outer.shape[1]
+    fetched = (
+        (w_outer, raw_mixer.at[0]), (w_inner, raw_mixer.at[1]), (w_value, raw_mixer.at[2]),
+        (w_mixout, raw_mixout), (w_gate, raw_gate), (w_upward, raw_up), (w_down, raw_down),
+    )
+
     def fetch(k):
-        source, target = ((w_gate, raw_gate), (w_upward, raw_up), (w_down, raw_down))[k]
-        return pltpu.make_async_copy(source, target, local_sem.at[6 + k])
-
-    for k in range(3):
+        return pltpu.make_async_copy(*fetched[k], local_sem.at[7 + k])
+
+    for k in range(len(fetched)):
         fetch(k).start()
     barrier = pltpu.get_barrier_semaphore()
     ring = [lax.rem(zed + step, DEPTH) * WIDTH + why for step in (1, DEPTH - 1)]
@@ -71,24 +77,35 @@
         pl.semaphore_signal(barrier, inc=1, device_id={"fs": peer}, device_id_type=MESH)
     for peer in (sibling, across):
         pl.semaphore_signal(barrier, inc=1, device_id={"tp": peer}, device_id_type=MESH)
-    wide = w_outer.shape[1]
-    for k, w in enumerate((w_outer, w_inner, w_value)):
-        h_mixer[:, k * wide : (k + 1) * wide] = w[...].astype(bf16)
-    h_mixout[...] = w_mixout[...].astype(bf16)
+    for k in range(4):
+        fetch(k).wait()
+    for k in range(3):
+        h_mixer[:, k * wide : (k + 1) * wide] = raw_mixer[k].astype(bf16)
+    h_mixout[...] = raw_mixout[...].astype(bf16)
     for k, row in enumerate((s_mixout, s_down)):
         h_scales[k * 8 : (k + 1) * 8, :] = jnp.broadcast_to(row[...], (8, row.shape[1]))
     pl.semaphore_wait(barrier, 5)
 
-    fulls = (scales, mixer, mixout, gated, back)
-    own_src = (h_scales, h_mixer, h_mixout, h_gated.at[why], h_back.at[why])
+    fulls = (scales, mixer, mixout, lead, rest, back)
+    split = (h_lead, h_rest, h_back)
+    own_src = (h_scales, h_mixer, h_mixout, *[h.at[why] for h in split])
 
     def place(p, owner):
-        if p in (MIXER, GATED):
+        if p in (MIXER, LEAD, REST):
             height = own_src[p].shape[0]
             return fulls[p].at[pl.ds(pl.multiple_of(owner * height, height), height), :]
         height, wide = own_src[p].shape
         first = pl.multiple_of(tp * height, height) if p == MIXOUT else 0
         return fulls[p].at[pl.ds(first, height), pl.ds(pl.multiple_of(owner * wide, wide), wide)]
+
+    first_own = LEAD * DEPTH - LEAD
+
+    def kind(p, owner):
+        return p if p < LEAD else LEAD + (p - LEAD) * WIDTH + lax.rem(owner, WIDTH)
+
+    def line_of(owner, way):
+        z = lax.div(owner, WIDTH)
+        return z if way == UP else lax.select(z == zed, DEPTH, z)
 
     def z_copy(p, owner, way, src=None):
         spot = place(p, owner)
@@ -96,7 +113,7 @@
         return pltpu.make_async_remote_copy(
             src_ref=spot if src is None else src,
             dst_ref=spot,
-            send_sem=z_send.at[p, owner, way],
+            send_sem=z_send.at[kind(p, owner), line_of(owner, way)],
             recv_sem=fs_recv.at[p, owner],
             device_id={"fs": (zed + step) * WIDTH + why},
             device_id_type=MESH,
@@ -107,7 +124,7 @@
         return pltpu.make_async_remote_copy(
             src_ref=spot if src is None else src,
             dst_ref=spot,
-            send_sem=y_send.at[p, owner],
+            send_sem=y_send.at[p * DEPTH + lax.div(owner, WIDTH) if p < LEAD else first_own + p],
             recv_sem=fs_recv.at[p, owner],
             device_id={"fs": beside},
             device_id_type=MESH,
@@ -148,15 +165,15 @@
     def mx_copy(owner, k, src=None):
         line, target = ((tp, sibling), (tp, across), (across, sibling))[k]
         height, wide = h_mixout.shape
-        spot = mixout.at[
-            pl.ds(pl.multiple_of(line * height, height), height),
-            pl.ds(pl.multiple_of(owner * wide, wide), wide),
-        ]
+        columns = slice(None)
+        if owner is not None:
+            columns = pl.ds(pl.multiple_of(owner * wide, wide), wide)
+        spot = mixout.at[pl.ds(pl.multiple_of(line * height, height), height), columns]
         return pltpu.make_async_remote_copy(
             src_ref=spot if src is None else src,
             dst_ref=spot,
-            send_sem=mx_send.at[owner, k],
-            recv_sem=mx_recv.at[owner, k],
+            send_sem=mx_send.at[k],
+            recv_sem=mx_recv.at[0 if owner is None else owner] if k == 1 else mx_whole.at[k // 2],
             device_id={"tp": target},
             device_id_type=MESH,
         )
@@ -235,7 +252,7 @@
         tp_copy(a, 0).wait_recv()
         tp_copy(a, 2).wait_recv()
 
-    own_tokens = pltpu.make_async_copy(tokens, tp_slot(0, tp), local_sem.at[5])
+    own_tokens = pltpu.make_async_copy(tokens, tp_slot(0, tp), local_sem.at[6])
 
     for p in firsts:
         y_copy(p, me, own_src[p]).start()
@@ -249,45 +266,55 @@
     main = units // 128 * 128
     middle, after = pl.ds(main, 128), main + 128
 
+    cut = h_lead.shape[2] // 2
+
     def share_out(gate, up, write):
-        write(0, pl.ds(0, main), gate[:, :main])
-        write(0, pl.ds(after, main), up[:, :main])
-        write(1, pl.ds(0, main), gate[:, after:])
-        write(1, pl.ds(after, main), up[:, after:])
+        tail = main - cut
+        for half, first in enumerate((0, after)):
+            for k, source in enumerate((gate, up)):
+                write(0, half, pl.ds(k * cut, cut), source[:, pl.ds(first, cut)])
+                at = pl.ds(k * (tail + 128), tail)
+                write(1, half, at, source[:, pl.ds(first + cut, tail)])
         gate, up = gate[:, middle], up[:, middle]
         low = lax.broadcasted_iota(jnp.int32, gate.shape, 1) < 64
-        write(0, middle, jnp.where(low, gate, pltpu.roll(up, 64, 1)))
-        write(1, middle, jnp.where(low, pltpu.roll(gate, 64, 1), up))
-
-    def write_scale(half, lanes, values):
-        s_gated[half : half + 1, lanes] = values
-
-    def write_gated(half, lanes, values):
-        h_gated[half, :, lanes] = values.astype(bf16)
-
-    for k in range(3):
+        write(1, 0, pl.ds(tail, 128), jnp.where(low, gate, pltpu.roll(up, 64, 1)))
+        write(1, 1, pl.ds(tail, 128), jnp.where(low, pltpu.roll(gate, 64, 1), up))
+
+    def write_scale(target, half, lanes, values):
+        (s_lead, s_rest)[target][half : half + 1, lanes] = values[0:1]
+
+    def write_gated(target, half, lanes, values):
+        split[target][half, :, lanes] = values.astype(bf16)
+
+    for k in range(4, len(fetched)):
         fetch(k).wait()
     share_out(raw_gate, raw_up, write_gated)
     h_back[0] = raw_down[:units, :].astype(bf16)
     h_back[1, :main, :] = raw_down[after:, :].astype(bf16)
     h_back[1, main:, :] = raw_down[units:after, :].astype(bf16)
-    spread = [jnp.broadcast_to(row[...], (8, row.shape[1])) for row in (s_gate, s_upward)]
-    share_out(
-        *spread, lambda half, lanes, values: write_scale(half, lanes, values[0:1])
-    )
-    for p in (GATED, BACK):
+    for k, row in enumerate((s_gate, s_upward)):
+        raw_scale[k] = jnp.broadcast_to(row[...], raw_scale.shape[1:])
+    share_out(raw_scale.at[0], raw_scale.at[1], write_scale)
+    for p in (LEAD, REST, BACK):
         own(p).start()
     back[units:, :] = jnp.zeros((back.shape[0] - units, back.shape[1]), bf16)
+
+    @pl.when(outer)
+    def _():
+        for p in (LEAD, REST):
+            z_own(p, why, own_src[p])
 
     relay_first(1)
     tp_second(0)
     relay_first(2)
-    z_own(GATED, why, own_src[GATED])
+    pl.when(jnp.logical_not(outer))(lambda: z_own(LEAD, why, own_src[LEAD]))
     relay_first(3)
-    y_copy(GATED, me, h_gated.at[other]).start()
+    y_copy(LEAD, me, h_lead.at[other]).start()
+    y_copy(REST, me, h_rest.at[other]).start()
+    relay(LEAD, 1, why)
     for s in range(DEPTH):
         from_beside(s)
-    relay(GATED, 1, why)
+    relay(LEAD, 2, why)
     tp_finish(0)
     own_tokens.wait()
     for p in firsts:
@@ -324,20 +351,22 @@
         ).astype(bf16)
 
     tp_first(1)
-    relay(GATED, 2, why)
-    arrived(GATED, beside)
-    z_own(GATED, other, None)
+    arrived(LEAD, beside)
+    z_own(LEAD, other, None)
+    pl.when(jnp.logical_not(outer))(lambda: z_own(REST, why, own_src[REST]))
     for owner in range(DEPTH * WIDTH):
         mx_copy(owner, 1).wait_recv()
         mx_copy(owner, 2).start()
     tp_second(1)
-    relay(GATED, 1, other)
-    for owner in range(DEPTH * WIDTH):
-        mx_copy(owner, 0).wait_recv()
-        mx_copy(owner, 2).wait_recv()
+    relay(LEAD, 1, other)
+    mx_copy(None, 0).wait_recv()
+    mx_copy(None, 2).wait_recv()
     tp_finish(1)
     for k in range(3):
         tp_copy(0, k).wait_send()
+
+    arrived(REST, beside)
+    z_own(REST, other, None)
 
     feat = tokens.shape[1]
     quarter = count // TP
@@ -386,33 +415,76 @@
         act_copy(1, h).start()
 
     spread_act(0)
-    relay(GATED, 2, other)
+    relay(LEAD, 2, other)
+    relay(REST, 1, why)
     spread_act(1)
+    relay(REST, 2, why)
+    relay(REST, 1, other)
+
+    def sent(p, row):
+        owner = zed * WIDTH + row
+        pl.when(can_up)(lambda: z_copy(p, owner, UP).wait_send())
+        pl.when(can_down)(lambda: z_copy(p, owner, DOWN).wait_send())
+        for s in (1, 2):
+            low, high = (zed - s) * WIDTH + row, (zed + s) * WIDTH + row
+            pl.when((zed >= s) & can_up)(lambda: z_copy(p, low, UP).wait_send())
+            pl.when((zed + s <= last_z) & can_down)(lambda: z_copy(p, high, DOWN).wait_send())
+
+    for p in firsts:
+        sent(p, why)
+        y_copy(p, me).wait_send()
+        for s in (1, 2, 3):
+            low, high = (zed - s) * WIDTH + why, (zed + s) * WIDTH + why
+            pl.when(zed >= s)(lambda: y_copy(p, low).wait_send())
+            pl.when(zed + s <= last_z)(lambda: y_copy(p, high).wait_send())
+    for k in range(3):
+        mx_copy(None, k).wait_send()
+    for k in range(3):
+        tp_copy(1, k).wait_send()
+
+    for h in range(2):
+        act_copy(2, h).wait_recv()
+        act_copy(3, h).start()
+    relay(REST, 2, other)
     arrived(BACK, beside)
     own(BACK).wait()
     for row in range(WIDTH):
         z_own(BACK, row, None)
-    for h in range(2):
-        act_copy(2, h).wait_recv()
-        act_copy(3, h).start()
-    own(GATED).wait()
+    for p in (LEAD, REST):
+        own(p).wait()
     for row in (why, other):
         for s in (1, 2, 3):
-            settle(GATED, s, row)
-
-    def activate(first, steps):
-        @pl.loop(0, steps)
+            settle(LEAD, s, row)
+    for h in range(2):
+        act_copy(1, h).wait_recv()
+        act_copy(3, h).wait_recv()
+
+    def activate(weights, row_scales, first, write):
+        @pl.loop(0, tiles)
         def _(i):
             rows = pl.ds(pl.multiple_of(first + i * ROWS, ROWS), ROWS)
-            both = jnp.dot(act[rows, :], gated[...], preferred_element_type=f32)
-            both = both * s_gated[pl.ds(why, 1), :]
-            gate, up = both[:, :main], both[:, main + 128 :]
-            hidden[rows, :main] = (gate / (1.0 + jnp.exp(-gate)) * up).astype(bf16)
-            gate = both[:, main : main + 128]
-            up = pltpu.roll(gate, 64, 1)
-            rest = gate / (1.0 + jnp.exp(-gate)) * up
-            lane = lax.broadcasted_iota(jnp.int32, rest.shape, 1)
-            hidden[rows, main:] = jnp.where(lane < 64, rest, 0.0).astype(bf16)
+            both = jnp.dot(act[rows, :], weights[...], preferred_element_type=f32)
+            write(rows, both * row_scales[pl.ds(why, 1), :])
+
+    def gate_with(gate, up):
+        return gate / (1.0 + jnp.exp(-gate)) * up
+
+    def write_lead(rows, both):
+        hidden[rows, :cut] = gate_with(both[:, :cut], both[:, cut:]).astype(bf16)
+
+    def write_rest(rows, both):
+        tail = main - cut
+        hidden[rows, cut:main] = gate_with(both[:, :tail], both[:, tail + 128 :]).astype(bf16)
+        mixed_lanes = both[:, tail : tail + 128]
+        ends = gate_with(mixed_lanes, pltpu.roll(mixed_lanes, 64, 1))
+        lane = lax.broadcasted_iota(jnp.int32, ends.shape, 1)
+        hidden[rows, main:] = jnp.where(lane < 64, ends, 0.0).astype(bf16)
+
+    for half in (other, why):
+        activate(lead, s_lead, half * count, write_lead)
+    for row in (why, other):
+        for s in (1, 2, 3):
+            settle(REST, s, row)
 
     pieces = count // PIECE
 
@@ -427,7 +499,7 @@
         return pltpu.make_async_remote_copy(
             src_ref=part.at[j, row, piece(t), :],
             dst_ref=from_core.at[line, row, piece(t), :],
-            send_sem=core_send.at[line, row, t],
+            send_sem=core_send.at[line, row],
             recv_sem=core_recv.at[line, row, t],
             device_id={"tp": sibling},
             device_id_type=MESH,
@@ -444,18 +516,15 @@
             device_id_type=MESH,
         )
 
-    def last_copy(j, row, t):
+    def last_copy(j, row, q):
         return pltpu.make_async_remote_copy(
-            src_ref=part.at[j, row, piece(t), :],
-            dst_ref=from_x.at[row, piece(t), :],
-            send_sem=last_send.at[row, t],
-            recv_sem=last_recv.at[row, t],
+            src_ref=part.at[j, row, piece(why * pieces + q), :],
+            dst_ref=from_x.at[row, piece(q), :],
+            send_sem=last_send.at[row, q],
+            recv_sem=last_recv.at[row, q],
             device_id={"tp": across},
             device_id_type=MESH,
         )
-
-    def x_first(k, row):
-        return row == 0 and k < last_z
 
     def multiply(k, row, half):
         j = block_at(k)
@@ -483,38 +552,21 @@
                 core_copy(j, row, t).wait_recv()
                 total = added(j, row, t, from_core[line, row, piece(t), :])
                 part[j, row, piece(t), :] = total.astype(bf16)
-                if x_first(k, row):
-                    pl.when(ex != line)(lambda: last_copy(j, row, t).start())
-                elif half is other:
+                if half is other:
                     sum_copy(j, row, q).start()
 
     def stage_2(k, row):
         j = block_at(k)
-        line = lax.div(j, 2)
-        mine = core == lax.rem(j, 2)
-
-        def x_sums():
-            for half in (other, why):
-                for q in range(pieces):
-                    t = half * pieces + q
-                    last_copy(j, row, t).wait_recv()
-                    total = added(j, row, t, from_x[row, piece(t), :])
-                    part[j, row, piece(t), :] = total.astype(bf16)
-                    if half is other:
-                        sum_copy(j, row, q).start()
-
-        def y_sums():
+
+        @pl.when(core == lax.rem(j, 2))
+        def _():
+            line = lax.div(j, 2)
             for q in range(pieces):
                 t = why * pieces + q
                 sum_copy(j, row, q).wait_recv()
                 total = added(j, row, t, from_y[line, row, piece(q), :])
                 part[j, row, piece(t), :] = total.astype(bf16)
-                pl.when(ex != line)(lambda: last_copy(j, row, t).start())
-
-        if x_first(k, row):
-            pl.when(mine & (ex == line))(x_sums)
-        else:
-            pl.when(mine)(y_sums)
+                pl.when(ex != line)(lambda: last_copy(j, row, q).start())
 
     def stage_3(k, row):
         j = block_at(k)
@@ -525,43 +577,37 @@
             columns = pl.ds(row * wide, wide)
             for q in range(pieces):
                 t = why * pieces + q
-                if x_first(k, row):
-                    sum_copy(j, row, q).wait_recv()
-                    extra = from_y[lax.div(j, 2), row, piece(q), :]
-                else:
-                    last_copy(j, row, t).wait_recv()
-                    extra = from_x[row, piece(t), :]
+                last_copy(j, row, q).wait_recv()
                 kept = residual_own[piece(q), columns].astype(f32)
-                out[piece(q), columns] = (kept + added(j, row, t, extra)).astype(bf16)
-
-    for h in range(2):
-        act_copy(1, h).wait_recv()
-        act_copy(3, h).wait_recv()
-    activate(other * count, tiles)
+                total = added(j, row, t, from_x[row, piece(q), :])
+                out[piece(q), columns] = (kept + total).astype(bf16)
+
+    activate(rest, s_rest, other * count, write_rest)
     for row in range(WIDTH):
         relay(BACK, 1, row)
     for row in range(WIDTH):
         multiply(0, row, other)
         stage_1(0, row, other)
-    activate(base, tiles)
-    for row in range(WIDTH):
-        relay(BACK, 2, row)
+    activate(rest, s_rest, base, write_rest)
     for row in range(WIDTH):
         multiply(0, row, why)
         stage_1(0, row, why)
 
     order = [(k, row) for k in range(DEPTH) for row in range(WIDTH)]
     after_unit = {
-        3: ((stage_2, 1), (stage_2, 0)),
-        4: ((stage_2, 3),),
-        5: ((stage_2, 2), (stage_3, 1), (stage_3, 0)),
-        6: ((stage_2, 5), (stage_2, 4), (stage_3, 3)),
+        3: ((stage_2, 0), (stage_2, 1)),
+        4: ((stage_2, 2),),
+        5: ((stage_2, 3), (stage_2, 4)),
+        6: ((stage_2, 5), (stage_3, 0), (stage_3, 1)),
         7: (
-            (stage_2, 6), (stage_3, 2), (stage_2, 7), (stage_3, 5), (stage_3, 4), (stage_3, 6),
-            (stage_3, 7),
+            (stage_2, 6), (stage_2, 7), (stage_3, 2), (stage_3, 3), (stage_3, 4), (stage_3, 5),
+            (stage_3, 6), (stage_3, 7),
         ),
     }
     for u, (k, row) in enumerate(order):
+        if u == 2 * WIDTH:
+            for line in range(WIDTH):
+                relay(BACK, 2, line)
         if k:
             owner = block_at(k) * WIDTH + row
             pl.when(outer)(lambda: arrived(BACK, owner))
@@ -571,55 +617,32 @@
         for stage, unit in after_unit.get(u, ()):
             stage(*order[unit])
 
-    def sent(p, row):
-        owner = zed * WIDTH + row
-        pl.when(can_up)(lambda: z_copy(p, owner, UP).wait_send())
-        pl.when(can_down)(lambda: z_copy(p, owner, DOWN).wait_send())
-        for s in (1, 2):
-            low, high = (zed - s) * WIDTH + row, (zed + s) * WIDTH + row
-            pl.when((zed >= s) & can_up)(lambda: z_copy(p, low, UP).wait_send())
-            pl.when((zed + s <= last_z) & can_down)(lambda: z_copy(p, high, DOWN).wait_send())
-
-    for p in range(5):
-        sent(p, why)
+    for p in (LEAD, REST, BACK):
         y_copy(p, me).wait_send()
-        if p in (GATED, BACK):
-            sent(p, other)
-        else:
-            for s in (1, 2, 3):
-                low, high = (zed - s) * WIDTH + why, (zed + s) * WIDTH + why
-                pl.when(zed >= s)(lambda: y_copy(p, low).wait_send())
-                pl.when(zed + s <= last_z)(lambda: y_copy(p, high).wait_send())
-    for owner in range(DEPTH * WIDTH):
-        for k in range(3):
-            mx_copy(owner, k).wait_send()
-    for k in range(3):
-        tp_copy(1, k).wait_send()
+        for row in range(WIDTH):
+            sent(p, row)
     for k in range(4):
         for h in range(2):
             act_copy(k, h).wait_send()
     for k, row in order:
         j = block_at(k)
-        line = lax.div(j, 2)
-        mine = core == lax.rem(j, 2)
 
         @pl.when(core != lax.rem(j, 2))
         def _():
-            for t in range(WIDTH * pieces):
-                core_copy(j, row, t).wait_send()
-
-        def sums_sent():
+            pltpu.make_async_remote_copy(
+                src_ref=part.at[j, row],
+                dst_ref=from_core.at[lax.div(j, 2), row],
+                send_sem=core_send.at[lax.div(j, 2), row],
+                recv_sem=core_recv.at[lax.div(j, 2), row, 0],
+                device_id={"tp": sibling},
+                device_id_type=MESH,
+            ).wait_send()
+
+        @pl.when(core == lax.rem(j, 2))
+        def _():
             for q in range(pieces):
                 sum_copy(j, row, q).wait_send()
-
-        def lasts_sent(halves):
-            for half in halves:
-                for q in range(pieces):
-                    last_copy(j, row, half * pieces + q).wait_send()
-
-        first = x_first(k, row)
-        pl.when(mine & (ex == line) if first else mine)(sums_sent)
-        pl.when(mine & (ex != line))(lambda: lasts_sent((other, why) if first else (why,)))
+                pl.when(ex != lax.div(j, 2))(lambda: last_copy(j, row, q).wait_send())
 
 
 def fused_device(
@@ -650,29 +673,36 @@
     cols = w_down.shape[1]
     half = units // 2
     padded = half // 128 * 128 + 128
+    cut = half // 128 * 3 // 5 * 128
     vmem = pl.BlockSpec(memory_space=pltpu.VMEM)
     hbm = pl.BlockSpec(memory_space=pl.ANY)
     dma = pltpu.SemaphoreType.DMA
     owners = DEPTH * WIDTH
     return pl.pallas_call(
         block_kernel,
-        out_shape=jax.ShapeDtypeStruct((count, feat), bf16),
-        in_specs=[hbm if k in (12, 13, 16) else vmem for k in range(18)],
+        out_shape=pltpu.VMEM((count, feat), bf16),
+        in_specs=[hbm if k in (0, 3, 4, 5, 10, 12, 13, 16) else vmem for k in range(18)],
         out_specs=vmem,
         scratch_shapes=[
             pltpu.VMEM((16, cols), jnp.float32),
             pltpu.VMEM((w_outer.shape[0], 3 * chan), bf16),
             pltpu.VMEM(w_mixout.shape, bf16),
-            pltpu.VMEM((2, w_gate.shape[0], units), bf16),
+            pltpu.VMEM((2, w_gate.shape[0], 2 * cut), bf16),
+            pltpu.VMEM((2, w_gate.shape[0], units - 2 * cut), bf16),
             pltpu.VMEM((2, half, cols), bf16),
-            pltpu.VMEM((2, units), jnp.float32),
+            pltpu.VMEM((2, 2 * cut), jnp.float32),
+            pltpu.VMEM((2, units - 2 * cut), jnp.float32),
             pltpu.VMEM(w_gate.shape, jnp.float32),
             pltpu.VMEM(w_upward.shape, jnp.float32),
             pltpu.VMEM(w_down.shape, jnp.float32),
+            pltpu.VMEM((3, *w_outer.shape), jnp.float32),
+            pltpu.VMEM(w_mixout.shape, jnp.float32),
+            pltpu.VMEM((2, 8, units), jnp.float32),
             pltpu.VMEM((WIDTH * count, model), bf16),
             pltpu.VMEM((model, 3 * chan), bf16),
             pltpu.VMEM((TP * chan, model), bf16),
-            pltpu.VMEM((model, units), bf16),
+            pltpu.VMEM((model, 2 * cut), bf16),
+            pltpu.VMEM((model, units - 2 * cut), bf16),
             pltpu.VMEM((padded, model), bf16),
             pltpu.VMEM((16, model), jnp.float32),
             pltpu.VMEM((count, TP * chan), bf16),
@@ -681,23 +711,24 @@
             pltpu.VMEM((DEPTH, WIDTH, WIDTH * count, cols), bf16),
             pltpu.VMEM((2, WIDTH, WIDTH * count, cols), bf16),
             pltpu.VMEM((2, WIDTH, count, cols), bf16),
-            pltpu.VMEM((WIDTH, WIDTH * count, cols), bf16),
-            dma((5, owners, 2)),
-            dma((5, owners)),
-            dma((5, owners)),
+            pltpu.VMEM((WIDTH, count, cols), bf16),
+            dma((9, DEPTH + 1)),
+            dma((3 * DEPTH + 3,)),
+            dma((6, owners)),
             dma((2, 3)),
             dma((2, 3)),
-            dma((owners, 3)),
-            dma((owners, 3)),
+            dma((3,)),
+            dma((owners,)),
+            dma((2,)),
             dma((4, 2)),
             dma((4, 2)),
-            dma((2, WIDTH, 4)),
+            dma((2, WIDTH)),
             dma((2, WIDTH, 4)),
             dma((2, WIDTH, 2)),
             dma((2, WIDTH, 2)),
-            dma((WIDTH, 4)),
-            dma((WIDTH, 4)),
-            dma((9,)),
+            dma((WIDTH, 2)),
+            dma((WIDTH, 2)),
+            dma((14,)),
         ],
         compiler_params=pltpu.CompilerParams(
             collective_id=0, has_side_effects=True, vmem_limit_bytes=62 * 1024 * 1024

time: 210 us -> 200 us (0.952)
  Pallas kernels: 208 us -> 199 us
    pallas_call x1, Pallas kernels: 208 us -> 199 us  [fused_device(): pl.pallas_call(block_kernel, out_shape=pltpu.VMEM((count, feat), bf16), i...]
where the time goes in v4:
time: 200 us
  Pallas kernels  199 us (100%)
    pallas_call x1, Pallas kernels, fused_device(): pl.pallas_call(block_kernel, out_shape=pltpu.VMEM((count, feat), bf16), i...  199 us

profile of v4, /device:TPU:3, one launch (start us, length us, event | category | flops | bytes accessed | tf_op | source)
XLA Modules:
  0.0 199.5 jit_solution(17034080569008683623)
XLA Ops:
  0.0 198.5 %shard_map.172 = bf16[1024,512]{1,0:T(8,128)(2,1)S(1)} custom-call(bf16[1024,512]{1,0:T(8,128)(2,1)} %tokens.1, f32[1,2048]{1,0:T(1,128)} %bitcast.2, f32[1,2048]{1,0:T(1,128)} %bitcast.3, f32[256,256]{1,0:T(8,128)} %w_outer.1, f32[256,256]{1,0:T(8,128)} %w_inner.1, f32[256,256]{1,0:T(8,128)} %w_value.1, f32[1,256]{1,0:T(1,128)} %s_outer.1, ...), custom_call_target="tpu_custom_call" | custom-call | tf_op jit(solution)/shard_map/pallas_call | solution.py:681
  198.5 1.0 copy.20

commit v5 on v4

--- a/solution.py
+++ b/solution.py
@@ -31,7 +31,7 @@
 ROWS = 256
 PIECE = 512
 UP, DOWN = 0, 1
-SCALES, MIXER, MIXOUT, LEAD, REST, BACK = range(6)
+SCALES, MIXER, MIXOUT, LEAD, REST, BACK, BACK_END = range(7)
 MESH = pl.DeviceIdType.MESH
 
 
@@ -39,7 +39,7 @@
     tokens, mixer_gain, ffn_gain, w_outer, w_inner, w_value, s_outer, s_inner, s_value, taps,
     w_mixout, s_mixout, w_gate, w_upward, s_gate, s_upward, w_down, s_down,
     out,
-    h_scales, h_mixer, h_mixout, h_lead, h_rest, h_back, s_lead, s_rest, raw_gate, raw_up, raw_down,
+    h_scales, h_mixer, h_mixout, h_lead, h_rest, h_back, h_back_end, s_lead, s_rest, raw_gate, raw_up, raw_down,
     raw_mixer, raw_mixout, raw_scale,
     act, mixer, mixout, lead, rest, back, scales, mixed, hidden, residual_own,
     part, from_core, from_y, from_x,
@@ -67,7 +67,7 @@
     )
 
     def fetch(k):
-        return pltpu.make_async_copy(*fetched[k], local_sem.at[7 + k])
+        return pltpu.make_async_copy(*fetched[k], local_sem.at[8 + k])
 
     for k in range(len(fetched)):
         fetch(k).start()
@@ -83,11 +83,11 @@
         h_mixer[:, k * wide : (k + 1) * wide] = raw_mixer[k].astype(bf16)
     h_mixout[...] = raw_mixout[...].astype(bf16)
     for k, row in enumerate((s_mixout, s_down)):
-        h_scales[k * 8 : (k + 1) * 8, :] = jnp.broadcast_to(row[...], (8, row.shape[1]))
+        h_scales[k * 4 : (k + 1) * 4, :] = jnp.broadcast_to(row[...], (4, row.shape[1]))
     pl.semaphore_wait(barrier, 5)
 
-    fulls = (scales, mixer, mixout, lead, rest, back)
-    split = (h_lead, h_rest, h_back)
+    fulls = (scales, mixer, mixout, lead, rest, back, back)
+    split = (h_lead, h_rest, h_back, h_back_end)
     own_src = (h_scales, h_mixer, h_mixout, *[h.at[why] for h in split])
 
     def place(p, owner):
@@ -96,7 +96,10 @@
             return fulls[p].at[pl.ds(pl.multiple_of(owner * height, height), height), :]
         height, wide = own_src[p].shape
         first = pl.multiple_of(tp * height, height) if p == MIXOUT else 0
-        return fulls[p].at[pl.ds(first, height), pl.ds(pl.multiple_of(owner * wide, wide), wide)]
+        start = owner * wide
+        if p >= BACK:
+            start = owner * 2 * wide + (p - BACK) * wide
+        return fulls[p].at[pl.ds(first, height), pl.ds(pl.multiple_of(start, wide), wide)]
 
     first_own = LEAD * DEPTH - LEAD
 
@@ -252,7 +255,7 @@
         tp_copy(a, 0).wait_recv()
         tp_copy(a, 2).wait_recv()
 
-    own_tokens = pltpu.make_async_copy(tokens, tp_slot(0, tp), local_sem.at[6])
+    own_tokens = pltpu.make_async_copy(tokens, tp_slot(0, tp), local_sem.at[7])
 
     for p in firsts:
         y_copy(p, me, own_src[p]).start()
@@ -289,13 +292,16 @@
     for k in range(4, len(fetched)):
         fetch(k).wait()
     share_out(raw_gate, raw_up, write_gated)
-    h_back[0] = raw_down[:units, :].astype(bf16)
-    h_back[1, :main, :] = raw_down[after:, :].astype(bf16)
-    h_back[1, main:, :] = raw_down[units:after, :].astype(bf16)
+    narrow = h_back.shape[2]
+    for k, target in enumerate((h_back, h_back_end)):
+        lanes = pl.ds(k * narrow, narrow)
+        target[0] = raw_down[:units, lanes].astype(bf16)
+        target[1, :main, :] = raw_down[after:, lanes].astype(bf16)
+        target[1, main:, :] = raw_down[units:after, lanes].astype(bf16)
     for k, row in enumerate((s_gate, s_upward)):
         raw_scale[k] = jnp.broadcast_to(row[...], raw_scale.shape[1:])
     share_out(raw_scale.at[0], raw_scale.at[1], write_scale)
-    for p in (LEAD, REST, BACK):
+    for p in (LEAD, REST, BACK, BACK_END):
         own(p).start()
     back[units:, :] = jnp.zeros((back.shape[0] - units, back.shape[1]), bf16)
 
@@ -408,6 +414,7 @@
                 act_copy(0, h).start()
 
     y_copy(BACK, me, h_back.at[other]).start()
+    y_copy(BACK_END, me, h_back_end.at[other]).start()
 
     def spread_act(h):
         act_copy(0, h).wait_recv()
@@ -446,10 +453,12 @@
         act_copy(2, h).wait_recv()
         act_copy(3, h).start()
     relay(REST, 2, other)
-    arrived(BACK, beside)
-    own(BACK).wait()
+    for p in (BACK, BACK_END):
+        arrived(p, beside)
+        own(p).wait()
     for row in range(WIDTH):
-        z_own(BACK, row, None)
+        for p in (BACK, BACK_END):
+            z_own(p, row, None)
     for p in (LEAD, REST):
         own(p).wait()
     for row in (why, other):
@@ -494,97 +503,122 @@
     def block_at(k):
         return lax.rem(zed + k * (1 - 2 * lax.div(zed, last_z)) + DEPTH, DEPTH)
 
-    def core_copy(j, row, t):
-        line = lax.div(j, 2)
+    def region(ref, half, q, by_columns):
+        if by_columns:
+            wide = h_back.shape[2]
+            return ref.at[pl.ds(pl.multiple_of(half * count, count), count), pl.ds(q * wide, wide)]
+        return ref.at[piece(half * pieces + q), :]
+
+    def core_copy(j, row, half, q, by_columns):
+        line, t = lax.div(j, 2), half * pieces + q
         return pltpu.make_async_remote_copy(
-            src_ref=part.at[j, row, piece(t), :],
-            dst_ref=from_core.at[line, row, piece(t), :],
+            src_ref=region(part.at[j, row], half, q, by_columns),
+            dst_ref=region(from_core.at[line, row], half, q, by_columns),
             send_sem=core_send.at[line, row],
             recv_sem=core_recv.at[line, row, t],
             device_id={"tp": sibling},
             device_id_type=MESH,
         )
 
-    def sum_copy(j, row, q):
+    def sum_copy(j, row, q, by_columns):
         line = lax.div(j, 2)
         return pltpu.make_async_remote_copy(
-            src_ref=part.at[j, row, piece(other * pieces + q), :],
-            dst_ref=from_y.at[line, row, piece(q), :],
+            src_ref=region(part.at[j, row], other, q, by_columns),
+            dst_ref=region(from_y.at[line, row], 0, q, by_columns),
             send_sem=sum_send.at[line, row, q],
             recv_sem=sum_recv.at[line, row, q],
             device_id={"fs": beside},
             device_id_type=MESH,
         )
 
-    def last_copy(j, row, q):
+    def last_copy(j, row, q, by_columns):
         return pltpu.make_async_remote_copy(
-            src_ref=part.at[j, row, piece(why * pieces + q), :],
-            dst_ref=from_x.at[row, piece(q), :],
+            src_ref=region(part.at[j, row], why, q, by_columns),
+            dst_ref=region(from_x.at[row], 0, q, by_columns),
             send_sem=last_send.at[row, q],
             recv_sem=last_recv.at[row, q],
             device_id={"tp": across},
             device_id_type=MESH,
         )
 
+    def is_last(k, row):
+        return k == last_z and row == WIDTH - 1
+
     def multiply(k, row, half):
         j = block_at(k)
-        wide = h_back.shape[2]
+        wide = 2 * h_back.shape[2]
         columns = pl.ds(pl.multiple_of((j * WIDTH + row) * wide, wide), wide)
 
         @pl.loop(0, pieces)
         def _(q):
             t = half * pieces + q
             term = jnp.dot(hidden[piece(t), :], back[:, columns], preferred_element_type=f32)
-            part[j, row, piece(t), :] = (term * scales[8:9, columns]).astype(bf16)
-            pl.when(core != lax.rem(j, 2))(lambda: core_copy(j, row, t).start())
-
-    def added(j, row, t, extra):
-        return part[j, row, piece(t), :].astype(f32) + extra.astype(f32)
-
-    def stage_1(k, row, half):
-        j = block_at(k)
-
-        @pl.when(core == lax.rem(j, 2))
-        def _():
-            line = lax.div(j, 2)
-            for q in range(pieces):
-                t = half * pieces + q
-                core_copy(j, row, t).wait_recv()
-                total = added(j, row, t, from_core[line, row, piece(t), :])
-                part[j, row, piece(t), :] = total.astype(bf16)
-                if half is other:
-                    sum_copy(j, row, q).start()
-
-    def stage_2(k, row):
-        j = block_at(k)
-
-        @pl.when(core == lax.rem(j, 2))
-        def _():
-            line = lax.div(j, 2)
-            for q in range(pieces):
-                t = why * pieces + q
-                sum_copy(j, row, q).wait_recv()
-                total = added(j, row, t, from_y[line, row, piece(q), :])
-                part[j, row, piece(t), :] = total.astype(bf16)
-                pl.when(ex != line)(lambda: last_copy(j, row, q).start())
-
-    def stage_3(k, row):
+            part[j, row, piece(t), :] = (term * scales[4:5, columns]).astype(bf16)
+            pl.when(core != lax.rem(j, 2))(lambda: core_copy(j, row, half, q, False).start())
+
+    def multiply_narrow(k, row, half, q):
         j = block_at(k)
         wide = h_back.shape[2]
+        start = (j * WIDTH + row) * 2 * wide + q * wide
+        columns = pl.ds(pl.multiple_of(start, wide), wide)
+
+        @pl.loop(0, pieces)
+        def _(i):
+            t = half * pieces + i
+            term = jnp.dot(hidden[piece(t), :], back[:, columns], preferred_element_type=f32)
+            part[j, row, piece(t), pl.ds(q * wide, wide)] = (
+                term * scales[4:5, columns]
+            ).astype(bf16)
+
+        pl.when(core != lax.rem(j, 2))(lambda: core_copy(j, row, half, q, True).start())
+
+    def added(j, row, half, q, by_columns, extra):
+        spot = region(part.at[j, row], half, q, by_columns)
+        return spot[...].astype(f32) + extra[...].astype(f32)
+
+    def stage_1(k, row, half, some=None):
+        j, by = block_at(k), is_last(k, row)
+
+        @pl.when(core == lax.rem(j, 2))
+        def _():
+            line = lax.div(j, 2)
+            for q in range(pieces) if some is None else (some,):
+                core_copy(j, row, half, q, by).wait_recv()
+                extra = region(from_core.at[line, row], half, q, by)
+                total = added(j, row, half, q, by, extra)
+                region(part.at[j, row], half, q, by)[...] = total.astype(bf16)
+                if half is other:
+                    sum_copy(j, row, q, by).start()
+
+    def stage_2(k, row, some=None):
+        j, by = block_at(k), is_last(k, row)
+
+        @pl.when(core == lax.rem(j, 2))
+        def _():
+            line = lax.div(j, 2)
+            for q in range(pieces) if some is None else (some,):
+                sum_copy(j, row, q, by).wait_recv()
+                total = added(j, row, why, q, by, region(from_y.at[line, row], 0, q, by))
+                region(part.at[j, row], why, q, by)[...] = total.astype(bf16)
+                pl.when(ex != line)(lambda: last_copy(j, row, q, by).start())
+
+    def stage_3(k, row):
+        j, by = block_at(k), is_last(k, row)
+        wide = 2 * h_back.shape[2]
 
         @pl.when(tp == j)
         def _():
-            columns = pl.ds(row * wide, wide)
             for q in range(pieces):
-                t = why * pieces + q
-                last_copy(j, row, q).wait_recv()
-                kept = residual_own[piece(q), columns].astype(f32)
-                total = added(j, row, t, from_x[row, piece(q), :])
-                out[piece(q), columns] = (kept + total).astype(bf16)
+                last_copy(j, row, q, by).wait_recv()
+                total = added(j, row, why, q, by, region(from_x.at[row], 0, q, by))
+                lanes = pl.ds(row * wide, wide)
+                kept = region(residual_own.at[:, lanes], 0, q, by)[...].astype(f32)
+                region(out.at[:, lanes], 0, q, by)[...] = (kept + total).astype(bf16)
 
     activate(rest, s_rest, other * count, write_rest)
     for row in range(WIDTH):
-        relay(BACK, 1, row)
+        for p in (BACK, BACK_END):
+            relay(p, 1, row)
     for row in range(WIDTH):
         multiply(0, row, other)
         stage_1(0, row, other)
@@ -600,24 +634,34 @@
         5: ((stage_2, 3), (stage_2, 4)),
         6: ((stage_2, 5), (stage_3, 0), (stage_3, 1)),
         7: (
-            (stage_2, 6), (stage_2, 7), (stage_3, 2), (stage_3, 3), (stage_3, 4), (stage_3, 5),
+            (stage_2, 7), (stage_3, 2), (stage_3, 3), (stage_3, 4), (stage_3, 5),
             (stage_3, 6), (stage_3, 7),
         ),
     }
     for u, (k, row) in enumerate(order):
         if u == 2 * WIDTH:
             for line in range(WIDTH):
-                relay(BACK, 2, line)
+                for p in (BACK, BACK_END):
+                    relay(p, 2, line)
         if k:
             owner = block_at(k) * WIDTH + row
-            pl.when(outer)(lambda: arrived(BACK, owner))
-            for half in (other, why):
-                multiply(k, row, half)
-                stage_1(k, row, half)
+            if is_last(k, row):
+                for q in range(pieces):
+                    pl.when(outer)(lambda: arrived(BACK + q, owner))
+                    for half in (other, why):
+                        multiply_narrow(k, row, half, q)
+                        stage_1(k, row, half, q)
+                    stage_2(*order[u - 1], q)
+            else:
+                for p in (BACK, BACK_END):
+                    pl.when(outer)(lambda: arrived(p, owner))
+                for half in (other, why):
+                    multiply(k, row, half)
+                    stage_1(k, row, half)
         for stage, unit in after_unit.get(u, ()):
             stage(*order[unit])
 
-    for p in (LEAD, REST, BACK):
+    for p in (LEAD, REST, BACK, BACK_END):
         y_copy(p, me).wait_send()
         for row in range(WIDTH):
             sent(p, row)
@@ -641,8 +685,9 @@
         @pl.when(core == lax.rem(j, 2))
         def _():
             for q in range(pieces):
-                sum_copy(j, row, q).wait_send()
-                pl.when(ex != lax.div(j, 2))(lambda: last_copy(j, row, q).wait_send())
+                by = is_last(k, row)
+                sum_copy(j, row, q, by).wait_send()
+                pl.when(ex != lax.div(j, 2))(lambda: last_copy(j, row, q, by).wait_send())
 
 
 def fused_device(
@@ -673,7 +718,7 @@
     cols = w_down.shape[1]
     half = units // 2
     padded = half // 128 * 128 + 128
-    cut = half // 128 * 3 // 5 * 128
+    cut = half // 128 * 4 // 5 * 128
     vmem = pl.BlockSpec(memory_space=pltpu.VMEM)
     hbm = pl.BlockSpec(memory_space=pl.ANY)
     dma = pltpu.SemaphoreType.DMA
@@ -684,12 +729,13 @@
         in_specs=[hbm if k in (0, 3, 4, 5, 10, 12, 13, 16) else vmem for k in range(18)],
         out_specs=vmem,
         scratch_shapes=[
-            pltpu.VMEM((16, cols), jnp.float32),
+            pltpu.VMEM((8, cols), jnp.float32),
             pltpu.VMEM((w_outer.shape[0], 3 * chan), bf16),
             pltpu.VMEM(w_mixout.shape, bf16),
             pltpu.VMEM((2, w_gate.shape[0], 2 * cut), bf16),
             pltpu.VMEM((2, w_gate.shape[0], units - 2 * cut), bf16),
-            pltpu.VMEM((2, half, cols), bf16),
+            pltpu.VMEM((2, half, cols // 2), bf16),
+            pltpu.VMEM((2, half, cols // 2), bf16),
             pltpu.VMEM((2, 2 * cut), jnp.float32),
             pltpu.VMEM((2, units - 2 * cut), jnp.float32),
             pltpu.VMEM(w_gate.shape, jnp.float32),
@@ -704,7 +750,7 @@
             pltpu.VMEM((model, 2 * cut), bf16),
             pltpu.VMEM((model, units - 2 * cut), bf16),
             pltpu.VMEM((padded, model), bf16),
-            pltpu.VMEM((16, model), jnp.float32),
+            pltpu.VMEM((8, model), jnp.float32),
             pltpu.VMEM((count, TP * chan), bf16),
             pltpu.VMEM((WIDTH * count, padded), bf16),
             pltpu.VMEM((count, feat), bf16),
@@ -712,9 +758,9 @@
             pltpu.VMEM((2, WIDTH, WIDTH * count, cols), bf16),
             pltpu.VMEM((2, WIDTH, count, cols), bf16),
             pltpu.VMEM((WIDTH, count, cols), bf16),
-            dma((9, DEPTH + 1)),
-            dma((3 * DEPTH + 3,)),
-            dma((6, owners)),
+            dma((11, DEPTH + 1)),
+            dma((3 * DEPTH + 4,)),
+            dma((7, owners)),
             dma((2, 3)),
             dma((2, 3)),
             dma((3,)),
@@ -728,7 +774,7 @@
             dma((2, WIDTH, 2)),
             dma((WIDTH, 2)),
             dma((WIDTH, 2)),
-            dma((14,)),
+            dma((15,)),
         ],
         compiler_params=pltpu.CompilerParams(
             collective_id=0, has_side_effects=True, vmem_limit_bytes=62 * 1024 * 1024

time: 200 us -> 198 us (0.990)
  Pallas kernels: 199 us -> 197 us
where the time goes in v5:
time: 198 us
  Pallas kernels  197 us (99%)
    pallas_call x1, Pallas kernels, fused_device(): pl.pallas_call(block_kernel, out_shape=pltpu.VMEM((count, feat), bf16), i...  197 us

profile of v5, /device:TPU:3, one launch (start us, length us, event | category | flops | bytes accessed | tf_op | source)
XLA Modules:
  0.0 197.8 jit_solution(17942002120831910482)
XLA Ops:
  0.0 196.8 %shard_map.172 = bf16[1024,512]{1,0:T(8,128)(2,1)S(1)} custom-call(bf16[1024,512]{1,0:T(8,128)(2,1)} %tokens.1, f32[1,2048]{1,0:T(1,128)} %bitcast.2, f32[1,2048]{1,0:T(1,128)} %bitcast.3, f32[256,256]{1,0:T(8,128)} %w_outer.1, f32[256,256]{1,0:T(8,128)} %w_inner.1, f32[256,256]{1,0:T(8,128)} %w_value.1, f32[1,256]{1,0:T(1,128)} %s_outer.1, ...), custom_call_target="tpu_custom_call" | custom-call | tf_op jit(solution)/shard_map/pallas_call | solution.py:726
  196.8 1.0 copy.20

commit v6 on v5

--- a/solution.py
+++ b/solution.py
@@ -36,16 +36,17 @@
 
 
 def block_kernel(
-    tokens, mixer_gain, ffn_gain, w_outer, w_inner, w_value, s_outer, s_inner, s_value, taps,
-    w_mixout, s_mixout, w_gate, w_upward, s_gate, s_upward, w_down, s_down,
+    tokens, g_mixer, g_ffn, w_outer, w_inner, w_value, g_outer, g_inner, g_value, g_taps,
+    w_mixout, g_mixout, w_gate, w_upward, g_gate, g_upward, w_down, g_down,
     out,
     h_scales, h_mixer, h_mixout, h_lead, h_rest, h_back, h_back_end, s_lead, s_rest, raw_gate, raw_up, raw_down,
     raw_mixer, raw_mixout, raw_scale,
+    mixer_gain, ffn_gain, s_outer, s_inner, s_value, taps, s_mixout, s_gate, s_upward, s_down,
     act, mixer, mixout, lead, rest, back, scales, mixed, hidden, residual_own,
     part, from_core, from_y, from_x,
     z_send, y_send, fs_recv, tp_send, tp_recv, mx_send, mx_recv, mx_whole,
     act_send, act_recv, core_send, core_recv, sum_send, sum_recv, last_send, last_recv,
-    local_sem,
+    local_sem, small_sem,
 ):
     f32, bf16 = jnp.float32, jnp.bfloat16
     me, tp = lax.axis_index("fs"), lax.axis_index("tp")
@@ -69,7 +70,20 @@
     def fetch(k):
         return pltpu.make_async_copy(*fetched[k], local_sem.at[8 + k])
 
-    for k in range(len(fetched)):
+    small = (
+        (g_mixout, s_mixout), (g_down, s_down), (g_gate, s_gate), (g_upward, s_upward),
+        (g_mixer, mixer_gain), (g_ffn, ffn_gain), (g_outer, s_outer), (g_inner, s_inner),
+        (g_value, s_value), (g_taps, taps),
+    )
+
+    def fetch_small(k):
+        return pltpu.make_async_copy(*small[k], small_sem.at[k])
+
+    for k in range(4):
+        fetch(k).start()
+    for k in range(len(small)):
+        fetch_small(k).start()
+    for k in range(4, len(fetched)):
         fetch(k).start()
     barrier = pltpu.get_barrier_semaphore()
     ring = [lax.rem(zed + step, DEPTH) * WIDTH + why for step in (1, DEPTH - 1)]
@@ -82,6 +96,8 @@
     for k in range(3):
         h_mixer[:, k * wide : (k + 1) * wide] = raw_mixer[k].astype(bf16)
     h_mixout[...] = raw_mixout[...].astype(bf16)
+    for k in range(2):
+        fetch_small(k).wait()
     for k, row in enumerate((s_mixout, s_down)):
         h_scales[k * 4 : (k + 1) * 4, :] = jnp.broadcast_to(row[...], (4, row.shape[1]))
     pl.semaphore_wait(barrier, 5)
@@ -291,6 +307,8 @@
 
     for k in range(4, len(fetched)):
         fetch(k).wait()
+    for k in range(2, len(small)):
+        fetch_small(k).wait()
     share_out(raw_gate, raw_up, write_gated)
     narrow = h_back.shape[2]
     for k, target in enumerate((h_back, h_back_end)):
@@ -726,7 +744,7 @@
     return pl.pallas_call(
         block_kernel,
         out_shape=pltpu.VMEM((count, feat), bf16),
-        in_specs=[hbm if k in (0, 3, 4, 5, 10, 12, 13, 16) else vmem for k in range(18)],
+        in_specs=[hbm] * 18,
         out_specs=vmem,
         scratch_shapes=[
             pltpu.VMEM((8, cols), jnp.float32),
@@ -744,6 +762,14 @@
             pltpu.VMEM((3, *w_outer.shape), jnp.float32),
             pltpu.VMEM(w_mixout.shape, jnp.float32),
             pltpu.VMEM((2, 8, units), jnp.float32),
+            *[
+                pltpu.VMEM(row, jnp.float32)
+                for row in (
+                    (1, model), (1, model), scale_outer.shape, scale_inner.shape,
+                    scale_value.shape, conv_taps.shape, scale_mixout.shape, scale_gate.shape,
+                    scale_upward.shape, scale_down.shape,
+                )
+            ],
             pltpu.VMEM((WIDTH * count, model), bf16),
             pltpu.VMEM((model, 3 * chan), bf16),
             pltpu.VMEM((TP * chan, model), bf16),
@@ -775,6 +801,7 @@
             dma((WIDTH, 2)),
             dma((WIDTH, 2)),
             dma((15,)),
+            dma((10,)),
         ],
         compiler_params=pltpu.CompilerParams(
             collective_id=0, has_side_effects=True, vmem_limit_bytes=62 * 1024 * 1024

time: 198 us -> 197 us (level)
  no operation moved by 1% of the time
where the time goes in v6:
time: 197 us
  Pallas kernels  196 us (99%)
    pallas_call x1, Pallas kernels, fused_device(): pl.pallas_call(block_kernel, out_shape=pltpu.VMEM((count, feat), bf16), i...  196 us

profile of v6, /device:TPU:3, one launch (start us, length us, event | category | flops | bytes accessed | tf_op | source)
XLA Modules:
  0.0 197.1 jit_solution(15516179494570941834)
XLA Ops:
  0.0 196.1 %shard_map.172 = bf16[1024,512]{1,0:T(8,128)(2,1)S(1)} custom-call(bf16[1024,512]{1,0:T(8,128)(2,1)} %tokens.1, f32[1,2048]{1,0:T(1,128)} %bitcast.2, f32[1,2048]{1,0:T(1,128)} %bitcast.3, f32[256,256]{1,0:T(8,128)} %w_outer.1, f32[256,256]{1,0:T(8,128)} %w_inner.1, f32[256,256]{1,0:T(8,128)} %w_value.1, f32[1,256]{1,0:T(1,128)} %g_outer.1, ...), custom_call_target="tpu_custom_call" | custom-call | tf_op jit(solution)/shard_map/pallas_call | solution.py:744
  196.1 1.0 copy.20
